TPU v7x, 256 devices: a whole 4x4x8 slice. The times are simulated.
256 devices in a mesh: ep: 16 (over y, x), tp: 16 (over z, core).
Axes of the slice: x: 4, y: 4, z: 8, core: 2. Of those that a mesh axis runs over, the one named last changes fastest.
Arguments:
- query_rows: bfloat16 [16384, 2048], P('ep', 'tp'), may hold values from -6 to 6
- key_rows: bfloat16 [16384, 2048], P('ep', 'tp'), may hold values from -6 to 6
- value_rows: bfloat16 [16384, 4096], P('ep', 'tp'), may hold values from -6 to 6
- gate_rows: bfloat16 [16384, 4096], P('ep', 'tp'), may hold values from -6 to 6
- log_decay: float32 [16, 16384], P('tp', 'ep'), may hold values from -1.5 to 0
- out_weight: bfloat16 [4096, 2048], P('tp'), may hold values from -0.09375 to 0.09375
- channel_input: bfloat16 [12288, 2048], P(('ep', 'tp')), may hold values from -6 to 6
- norm_gain: float32 [2048], replicated, may hold values from 0.1 to 1.9
- routes: int32 [12288, 2], P(('ep', 'tp')), may hold values from 0 to 31, all different within a row; in each aligned block of 48 rows (0 to 47, 48 to 95, ...) at most 5 rows name the same one
- route_weight: float32 [12288, 2], P(('ep', 'tp')), may hold values from 0.2 to 1.5
- expert_gate: bfloat16 [32, 2048, 2048], P('ep', None, 'tp'), may hold values from -0.125 to 0.125
- expert_up: bfloat16 [32, 2048, 2048], P('ep', None, 'tp'), may hold values from -0.125 to 0.125
- expert_down: bfloat16 [32, 2048, 2048], P('ep', 'tp'), may hold values from -0.125 to 0.125
- shared_gate: bfloat16 [2048, 2048], P(None, 'tp'), may hold values from -0.125 to 0.125
- shared_up: bfloat16 [2048, 2048], P(None, 'tp'), may hold values from -0.125 to 0.125
- shared_down: bfloat16 [2048, 2048], P('tp'), may hold values from -0.125 to 0.125
Outputs:
- mixer_out: bfloat16 [16384, 2048], P(('ep', 'tp'))
- channel_out: bfloat16 [12288, 2048], P(('ep', 'tp'))
Inputs may be any that keep to these rules, and one draw needn't show every extreme that they name: `routes`: each row names 2 different experts; among the rows of one device no expert is named more than 5 times, a bound that some block reaches.
All inputs are finite; a program needn't handle non-finite values.
Results may differ from a plain program's by a relative error of at most 0.02.
Values may be sent and summed in bfloat16 or wider, within the bound.
A program may use at most 128 MiB of HBM per device.

v0:
```python
import jax
import jax.numpy as jnp
from jax import lax
from jax.sharding import Mesh
from jax.sharding import PartitionSpec as P

BLOCK = 128
EP = ("ep_0", "ep_1")
EP_TP = ("ep_0", "ep_1", "tp")


epsilon = 1e-06
turn_base = 10000.0


def filled_with(array, identity):
    return jax.tree.map(
        lambda a, e: jnp.broadcast_to(jnp.asarray(e, a.dtype), a.shape), array, identity
    )


def carried_in(array, axes, combine, identity):
    before = start = filled_with(array, identity)
    total = array
    for axis in reversed(axes):
        length, index = (lax.axis_size(axis), lax.axis_index(axis))
        pieces = jax.tree.map(
            lambda part, kind: lax.all_gather(part.astype(kind), axis),
            total,
            (jnp.bfloat16, jnp.bfloat16),
        )
        inside, total = (start, start)
        for k in range(length):
            passed = k < index
            total = combine(
                total, jax.tree.map(lambda part, own: part[k].astype(own.dtype), pieces, array)
            )
            inside = jax.tree.map(lambda new, old: jnp.where(passed, new, old), total, inside)
        before = combine(inside, before)
    return before


def turn_heads(rows, position):
    half_width = rows.shape[-1] // 2
    inverse = turn_base ** (-jnp.arange(half_width, dtype=jnp.float32) / half_width)
    angles = position[:, None] * inverse[None, :]
    cosine = jnp.cos(angles)[:, None, :]
    sine = jnp.sin(angles)[:, None, :]
    widened = rows.astype(jnp.float32)
    first_half = widened[..., :half_width]
    second_half = widened[..., half_width:]
    turned = jnp.concatenate(
        [first_half * cosine - second_half * sine, second_half * cosine + first_half * sine],
        axis=-1,
    )
    return turned.astype(jnp.bfloat16)


def chain_states(earlier, later):
    return (earlier[0] + later[0], jnp.exp(later[0])[:, None, None] * earlier[1] + later[1])


def compute_slots(route_rows, expert_count, capacity):
    flat_routes = route_rows.reshape(-1)
    onehot = (flat_routes[:, None] == jnp.arange(expert_count, dtype=jnp.int32)[None, :]).astype(
        jnp.int32
    )
    earlier = jnp.cumsum(onehot, axis=0) - onehot
    ranking = jnp.sum(earlier * onehot, axis=1)
    return flat_routes * capacity + ranking


def dispatch_matrix(slot_flat, tokens_here, topk_count, slot_count):
    hits = jnp.arange(slot_count, dtype=jnp.int32)[:, None] == slot_flat[None, :]
    return jnp.any(hits.reshape(slot_count, tokens_here, topk_count), axis=2).astype(jnp.bfloat16)


def gated_pair(gate_part, up_part):
    return (jax.nn.silu(gate_part) * up_part).astype(jnp.bfloat16)


def local(
    query_rows,
    key_rows,
    value_rows,
    gate_rows,
    log_decay,
    out_weight,
    channel_input,
    norm_gain,
    routes,
    route_weight,
    expert_gate,
    expert_up,
    expert_down,
    shared_gate,
    shared_up,
    shared_down,
):
    tokens_dev = query_rows.shape[0]
    head_count = log_decay.shape[0]
    key_width = query_rows.shape[1] // head_count
    value_width = value_rows.shape[1] // head_count
    block_count = tokens_dev // BLOCK
    position = (lax.axis_index(EP) * tokens_dev + jnp.arange(tokens_dev, dtype=jnp.int32)).astype(
        jnp.float32
    )
    queries = turn_heads(query_rows.reshape(tokens_dev, head_count, key_width), position)
    queries = queries.reshape(block_count, BLOCK, head_count, key_width)
    keys_turned = turn_heads(key_rows.reshape(tokens_dev, head_count, key_width), position)
    keys_turned = keys_turned.reshape(block_count, BLOCK, head_count, key_width)
    values = value_rows.reshape(block_count, BLOCK, head_count, value_width)
    decay = jnp.transpose(log_decay.reshape(head_count, block_count, BLOCK), (1, 2, 0))
    running = jnp.cumsum(decay, axis=1)
    block_end = running[:, -1, :]
    tail = jnp.exp(block_end[:, None, :] - running)
    value_wide = values.astype(jnp.float32)
    updates = jnp.einsum(
        "njhk,njhe->nhke", keys_turned.astype(jnp.float32) * tail[..., None], value_wide
    )

    def advance(carry, inputs):
        block_decay, update = inputs
        return (jnp.exp(block_decay)[:, None, None] * carry + update, carry)

    start_state = jnp.zeros((head_count, key_width, value_width), jnp.float32)
    final_state, state_before = lax.scan(advance, start_state, (block_end, updates))
    device_total = jnp.sum(block_end, axis=0)
    entry_parts = carried_in(
        (device_total, final_state),
        EP,
        chain_states,
        (jnp.zeros_like(device_total), jnp.zeros_like(final_state)),
    )
    entry_state = entry_parts[1]
    offsets = jnp.cumsum(block_end, axis=0) - block_end
    state_before = state_before + jnp.exp(offsets)[:, :, None, None] * entry_state[None]
    scores = jnp.einsum("nihk,njhk->nhij", queries, keys_turned, preferred_element_type=jnp.float32)
    by_head = jnp.transpose(running, (0, 2, 1))
    spread = by_head[:, :, :, None] - by_head[:, :, None, :]
    lower = jnp.arange(BLOCK)[:, None] >= jnp.arange(BLOCK)[None, :]
    weights = jnp.where(lower, scores * jnp.exp(jnp.where(lower, spread, 0.0)), 0.0).astype(
        jnp.bfloat16
    )
    retained = jnp.einsum("nhij,njhe->nihe", weights, values, preferred_element_type=jnp.float32)
    query_wide = queries.astype(jnp.float32)
    retained = retained + jnp.einsum(
        "nihk,nhke->nihe", query_wide * jnp.exp(running)[..., None], state_before
    )
    retained = retained.reshape(tokens_dev, head_count, value_width)
    scaled = retained * lax.rsqrt(jnp.mean(retained * retained, axis=-1, keepdims=True) + epsilon)
    gate_wide = gate_rows.astype(jnp.float32).reshape(tokens_dev, head_count, value_width)
    gated = (
        (jax.nn.silu(gate_wide) * scaled)
        .astype(jnp.bfloat16)
        .reshape(tokens_dev, head_count * value_width)
    )
    tokens_here = channel_input.shape[0]
    topk_count = routes.shape[1]
    model_width = channel_input.shape[1]
    local_experts = expert_gate.shape[0]
    hidden_part = expert_gate.shape[2]
    ep_count = lax.axis_size(EP)
    tp_count = lax.axis_size("tp")
    experts_all = ep_count * local_experts
    capacity = tokens_here * topk_count // experts_all + max(
        2, tokens_here * topk_count // (3 * experts_all)
    )
    slot_count = experts_all * capacity
    widened = channel_input.astype(jnp.float32)
    normed = (
        widened
        * lax.rsqrt(jnp.mean(widened * widened, axis=-1, keepdims=True) + epsilon)
        * norm_gain
    ).astype(jnp.bfloat16)
    own_slots = compute_slots(routes, experts_all, capacity)
    placing = dispatch_matrix(own_slots, tokens_here, topk_count, slot_count)
    outgoing = jnp.dot(placing, normed, preferred_element_type=jnp.float32).astype(jnp.bfloat16)
    outgoing = outgoing.reshape(experts_all, capacity, model_width)
    arrived = lax.all_to_all(outgoing, EP, split_axis=0, concat_axis=0, tiled=True)
    arrived = arrived.reshape(1, ep_count, local_experts, capacity, model_width)
    routed_piece, own_piece = lax.all_gather((arrived, normed[None]), "tp", axis=0, tiled=True)
    count = routed_piece.shape[0]
    routed_gate = jnp.einsum(
        "cejpd,jdf->cejpf", routed_piece, expert_gate, preferred_element_type=jnp.float32
    )
    routed_up = jnp.einsum(
        "cejpd,jdf->cejpf", routed_piece, expert_up, preferred_element_type=jnp.float32
    )
    routed_hidden = gated_pair(routed_gate, routed_up).reshape(count, slot_count, hidden_part)
    own_gate = jnp.einsum("cnd,df->cnf", own_piece, shared_gate, preferred_element_type=jnp.float32)
    own_up = jnp.einsum("cnd,df->cnf", own_piece, shared_up, preferred_element_type=jnp.float32)
    own_hidden = gated_pair(own_gate, own_up)
    hidden_all = jnp.concatenate([routed_hidden, own_hidden], axis=1)
    mixer_count = tokens_dev // tp_count
    mixer_term = jnp.dot(gated, out_weight, preferred_element_type=jnp.float32)
    mixer_term = mixer_term.reshape(lax.axis_size("tp") * 1, mixer_count, model_width)
    routed_hidden = hidden_all[:, :slot_count].reshape(
        lax.axis_size("tp") * 1, ep_count, local_experts, capacity, hidden_part
    )
    routed_term = jnp.einsum(
        "cejpf,jfd->cejpd", routed_hidden, expert_down, preferred_element_type=jnp.float32
    )
    routed_term = routed_term.reshape(lax.axis_size("tp") * 1, slot_count, model_width)
    shared_term = jnp.einsum(
        "cnf,fd->cnd", hidden_all[:, slot_count:], shared_down, preferred_element_type=jnp.float32
    )
    summed = lax.psum_scatter(
        jnp.concatenate([mixer_term, routed_term, shared_term], axis=1).astype(jnp.bfloat16),
        "tp",
        scatter_dimension=0,
        tiled=True,
    ).astype(jnp.float32)
    mixer_out = summed[0, :mixer_count].astype(jnp.bfloat16)
    routed_back = summed[0, mixer_count : mixer_count + slot_count].astype(jnp.bfloat16)
    routed_back = routed_back.reshape(experts_all, capacity, model_width)
    returned = lax.all_to_all(routed_back, EP, split_axis=0, concat_axis=0, tiled=True).reshape(
        slot_count, model_width
    )
    picked = jnp.take(returned, own_slots, axis=0).reshape(tokens_here, topk_count, model_width)
    shared_result = summed[0, mixer_count + slot_count :]
    channel = shared_result + jnp.sum(route_weight[:, :, None] * picked.astype(jnp.float32), axis=1)
    return (mixer_out, channel.astype(jnp.bfloat16))


def solution(mesh):
    split = Mesh(mesh.devices.reshape(4, 4, mesh.shape["tp"]), ("ep_0", "ep_1", "tp"))
    return jax.shard_map(
        local,
        mesh=split,
        in_specs=(
            P(EP, "tp"),
            P(EP, "tp"),
            P(EP, "tp"),
            P(EP, "tp"),
            P("tp", EP),
            P("tp", None),
            P(EP_TP, None),
            P(),
            P(EP_TP, None),
            P(EP_TP, None),
            P(EP, None, "tp"),
            P(EP, None, "tp"),
            P(EP, "tp", None),
            P(None, "tp"),
            P(None, "tp"),
            P("tp", None),
        ),
        out_specs=(P(EP_TP, None), P(EP_TP, None)),
        check_vma=False,
    )
```

profile of v0, /device:TPU:2, one launch (start us, length us, event | category | flops | bytes accessed | tf_op | source)
XLA Modules:
  0.0 375.6 jit_solution(7713296749920263441)
XLA Ops:
  7.2 1.1 fusion.55
  8.4 1.7 fusion.57
  10.2 0.8 copy.85
  11.7 0.7 compare_and_fusion
  12.5 1.3 convolution_convert_fusion.2
  14.1 23.2 %all_to_all.10 = bf16[32,5,2048]{2,1,0:T(8,128)(2,1)S(1)} all-to-all(bf16[32,5,2048]{2,1,0:T(8,128)(2,1)S(1)} %reshape.534), channel_id=1, replica_groups=mesh['ep_0'=4,'ep_1'=4,'tp'=16] {'ep_0','ep_1'}, dimensions={0} | all-to-all | bytes 1310720 | tf_op jit(solution)/shard_map/all_to_all | solution.py:180
  37.3 1.3 copy.88
  39.5 23.2 %fusion.93 = f32[8,128,1]{2,0,1:T(8,128)S(1)} fusion(f32[8,128,1]{2,0,1:T(8,128)S(1)} %copy.81), kind=kOutput, calls=%fused_computation.151 | output fusion | flops 130048 | bytes 8192 | tf_op jit(solution)/shard_map/jit(cumsum)/reduce_window_sum | solution.py:114
  62.8 0.7 slice_reduce_fusion
  63.4 1.3 dynamic-update-slice
  64.8 9.2 %all-reduce = bf16[4]{0:T(256)(128)(2,1)S(1)} all-reduce(bf16[4]{0:T(256)(128)(2,1)S(1)} %dynamic-update-slice), channel_id=1, replica_groups=mesh['ep_0'=4,'ep_1'=4,'tp'=16] {'ep_1'}, use_global_device_ids=true, to_apply=%add | all-reduce | flops 4 | bytes 16
  74.5 0.7 fusion.92
  75.2 1.3 dynamic-update-slice.1
  76.5 8.6 %all-reduce.1 = bf16[4]{0:T(256)(128)(2,1)S(1)} all-reduce(bf16[4]{0:T(256)(128)(2,1)S(1)} %dynamic-update-slice.1), channel_id=2, replica_groups=mesh['ep_0'=4,'ep_1'=4,'tp'=16] {'ep_0'}, use_global_device_ids=true, to_apply=%add.1 | all-reduce | flops 4 | bytes 16
  85.5 2.5 fusion.34
  88.0 1.6 convolution_bitcast_fusion.2
  89.7 15.8 %while.13 = (s32[]{:T(128)}, f32[1,128,256]{2,1,0:T(8,128)S(1)}, f32[8,1,128,256]{3,2,1,0:T(8,128)}, f32[8,1]{0,1:T(1,128)S(1)}, f32[8,1,128,256]{3,2,1,0:T(8,128)S(1)}, /*index=5*/s32[]{:T(128)}, s32[]{:T(128)}) while((s32[]{:T(128)}, f32[1,128,256]{2,1,0:T(8,128)S(1)}, f32[8,1,128,256]{3,2,1,0:T(8,128)}, f32[8,1]{0,1:T(1,128)S(1)}, ...), condition=%wide.region_2.3_spmd.clone, body=%wide.region_1.2_spmd.clone.sunk | while | flops 131075 | bytes 655980 | solution.py:127
  89.7 0.7 bitcast_dynamic-update-slice_fusion.2
  90.3 0.6 fusion.105
  91.0 0.7 bitcast_add_fusion.3
  91.7 0.7 bitcast_dynamic-update-slice_fusion.2
  92.3 0.6 fusion.105
  93.0 0.7 bitcast_add_fusion.3
  93.6 0.6 bitcast_dynamic-update-slice_fusion.2
  94.3 0.6 fusion.105
  94.9 0.7 bitcast_add_fusion.3
  95.6 0.7 bitcast_dynamic-update-slice_fusion.2
  96.9 0.7 bitcast_add_fusion.3
  97.6 0.7 bitcast_dynamic-update-slice_fusion.2
  98.2 0.6 fusion.105
  98.9 0.7 bitcast_add_fusion.3
  99.6 0.7 bitcast_dynamic-update-slice_fusion.2
  100.9 0.7 bitcast_add_fusion.3
  101.5 0.7 bitcast_dynamic-update-slice_fusion.2
  102.2 0.6 fusion.105
  102.8 0.7 bitcast_add_fusion.3
  103.5 0.7 bitcast_dynamic-update-slice_fusion.2
  104.8 0.7 bitcast_add_fusion.3
  105.5 0.7 slice_convert_fusion.3
  111.7 0.7 fusion.91
  115.2 11.0 %all-gather.1 = bf16[4,128,256]{2,1,0:T(8,128)(2,1)S(1)} all-gather(bf16[1,128,256]{2,1,0:T(8,128)(2,1)S(1)} %convert_element_type.229), channel_id=3, replica_groups=mesh['ep_0'=4,'ep_1'=4,'tp'=16] {'ep_1'}, dimensions={0}, use_global_device_ids=true | all-gather | bytes 327680 | tf_op jit(solution)/shard_map/all_gather | solution.py:28
  126.3 12.4 %all_gather.34 = bf16[4,1,128,256]{3,2,1,0:T(8,128)(2,1)S(1)} all-gather(bf16[1,1,128,256]{3,2,1,0:T(8,128)(2,1)S(1)} %fusion.73), channel_id=1, replica_groups=mesh['ep_0'=4,'ep_1'=4,'tp'=16] {'ep_0'}, dimensions={0}, use_global_device_ids=true | all-gather | bytes 327680 | tf_op jit(solution)/shard_map/all_gather | solution.py:28
  139.0 1.6 convolution_bitcast_fusion.3
  140.6 1.8 fusion.19
  142.8 1.3 convolution_convert_fusion
  144.1 4.3 %copy.90 = bf16[16,64,2048]{2,0,1:T(8,128)(2,1)} copy(bf16[16,64,2048]{2,1,0:T(8,128)(2,1)S(1)} %convolution_convert_fusion) | data formatting | bytes 8388608 | tf_op jit(solution)/shard_map/convert.8
  148.4 2.9 fusion.44
  151.4 6.9 %convolution_convert_fusion.1 = bf16[16,48,2048]{2,1,0:T(8,128)(2,1)} fusion(bf16[16,48,2048]{2,1,0:T(8,128)(2,1)} %bitcast.164, bf16[128,2048]{1,0:T(8,128)(2,1)S(1)} %copy-done.6, bf16[2048,128]{1,0:T(8,128)(2,1)S(1)} %copy-done.7, f32[16,48,128]{2,1,0:T(8,128)S(1)} %fusion.44), kind=kOutput, calls=%fused_computation.7 | convolution fusion | flops 807469056 | bytes 7733248 | tf_op jit(solution)/shard_map/cnf,fd->cnd/dot_general | solution.py:205
  158.2 5.4 %copy.91 = bf16[16,48,2048]{2,0,1:T(8,128)(2,1)} copy(bf16[16,48,2048]{2,1,0:T(8,128)(2,1)} %convolution_convert_fusion.1) | data formatting | bytes 6291456 | tf_op jit(solution)/shard_map/convert.10
  163.6 6.0 %convolution_bitcast_fusion.1 = f32[16,16,2,5,128]{4,1,3,0,2:T(8,128)S(1)} fusion(bf16[16,16,2,5,2048]{4,1,3,0,2:T(8,128)(2,1)} %all-gather.6.cloned.1.call-done, bf16[2,2048,128]{2,1,0:T(8,128)(2,1)} %param.28), kind=kOutput, calls=%fused_computation.10 | convolution fusion | flops 1342177280 | bytes 12845056 | tf_op jit(solution)/shard_map/cejpd,jdf->cejpf/dot_general | solution.py:184
  169.6 15.5 %convert_bitcast_fusion = bf16[16,16,2,5,2048]{4,1,3,0,2:T(8,128)(2,1)} fusion(bf16[16,16,2,5,2048]{4,1,3,0,2:T(8,128)(2,1)} %all-gather.6.cloned.1.call-done, f32[16,16,2,5,128]{4,1,3,0,2:T(8,128)S(1)} %convolution_bitcast_fusion.1, bf16[2,128,2048]{2,1,0:T(8,128)(2,1)S(1)} %copy-done, bf16[2,2048,128]{2,1,0:T(8,128)(2,1)S(1)} %copy-done.2), kind=kOutput, calls=%fused_computation.5 | convolution fusion | flops 2691563520 | bytes 24379392 | tf_op jit(solution)/shard_map/cejpf,jfd->cejpd/dot_general | solution.py:201
  185.1 13.8 %copy.89 = bf16[16,16,2,5,2048]{4,0,3,2,1:T(8,128)(2,1)} copy(bf16[16,16,2,5,2048]{4,1,3,0,2:T(8,128)(2,1)} %convert_bitcast_fusion) | data formatting | bytes 20971520 | tf_op jit(solution)/shard_map/cejpf,jfd->cejpd/transpose | solution.py:201
  198.9 8.5 %pad_maximum_fusion = bf16[16,272,2048]{2,0,1:T(8,128)(2,1)S(1)} fusion(bf16[16,48,2048]{2,0,1:T(8,128)(2,1)} %copy.91, bf16[16,160,2048]{2,0,1:T(8,128)(2,1)} %bitcast.162, bf16[16,64,2048]{2,0,1:T(8,128)(2,1)} %copy.90), kind=kLoop, calls=%fused_computation.4 | loop fusion | flops 17825792 | bytes 35651584 | tf_op jit(solution)/shard_map/concatenate | solution.py:209
  207.4 24.4 %copy.92 = bf16[16,272,2048]{2,1,0:T(8,128)(2,1)} copy(bf16[16,272,2048]{2,0,1:T(8,128)(2,1)S(1)} %pad_maximum_fusion) | data formatting | bytes 35651584 | tf_op jit(solution)/shard_map/concatenate | solution.py:209
  231.8 0.7 copy-done.10
  232.7 106.6 %reduce-scatter.2.cloned.1.call-done = bf16[1,272,2048]{2,1,0:T(8,128)(2,1)} async-done(((bf16[16,272,2048]{2,1,0:T(8,128)(2,1)}), bf16[1,272,2048]{2,1,0:T(8,128)(2,1)}) %reduce-scatter.2.cloned.1.call-update) | async-done | bytes 1114128 | tf_op jit(solution)/shard_map/reduce_scatter | solution.py:208
  339.2 1.1 slice.128
  340.4 1.2 convert_element_type.248
  341.6 7.3 %all-to-all-start.1 = ((bf16[32,5,2048]{2,1,0:T(8,128)(2,1)}), bf16[32,5,2048]{2,1,0:T(8,128)(2,1)S(1)}, u32[]{:S(2)}, u32[]{:S(2)}) async-start(bf16[32,5,2048]{2,1,0:T(8,128)(2,1)} %convert_element_type.248), calls=%async_computation.2 | async-start | bytes 2097152 | tf_op jit(solution)/shard_map/all_to_all | solution.py:217
  349.1 1.7 slice_bitcast_fusion
  350.8 13.2 %all-to-all-done.1 = bf16[32,5,2048]{2,1,0:T(8,128)(2,1)S(1)} async-done(((bf16[32,5,2048]{2,1,0:T(8,128)(2,1)}), bf16[32,5,2048]{2,1,0:T(8,128)(2,1)S(1)}, u32[]{:S(2)}, u32[]{:S(2)}) %all-to-all-start.1) | async-done | bytes 655392 | tf_op jit(solution)/shard_map/all_to_all | solution.py:217
  364.2 0.8 gather_fusion
  365.3 2.0 multiply_reduce_fusion
  367.4 1.6 fusion.58
  (78 shorter events, 6.8 us)
Async XLA Ops:
  7.2 162.4 %copy-start = (bf16[2,128,2048]{2,1,0:T(8,128)(2,1)S(1)}, bf16[2,128,2048]{2,1,0:T(8,128)(2,1)}, u32[]{:S(2)}) copy-start(bf16[2,128,2048]{2,1,0:T(8,128)(2,1)} %param.30) | copy-start | bytes 3145732
  7.2 141.2 %all-gather.8.cloned.1.call-start = ((), (), s32[]{:S(2)}) async-start(), calls=%async_computation.5 | async-start | bytes 3342336 | tf_op jit(solution)/shard_map/all_gather | solution.py:182
  10.1 153.5 %all-gather.6.cloned.1.call-start = ((), (), s32[]{:S(2)}) async-start(), calls=%async_computation.3 | async-start | bytes 11141120 | tf_op jit(solution)/shard_map/all_gather | solution.py:182
  13.8 24.9 %copy-start.11 = (f32[1,1024]{1,0:T(1,128)S(1)}, f32[1,1024]{1,0:T(1,128)}, u32[]{:S(2)}) copy-start(f32[1,1024]{1,0:T(1,128)} %param.22) | copy-start | bytes 12292
  13.8 25.2 %copy-start.14 = (u32[256]{0:T(256)S(1)}, u32[256]{0:T(256)}, u32[]{:S(2)}) copy-start(u32[256]{0:T(256)} %constant.103) | copy-start | bytes 3076
  14.1 59.9 %copy-start.13 = (u32[256]{0:T(256)S(1)}, u32[256]{0:T(256)}, u32[]{:S(2)}) copy-start(u32[256]{0:T(256)} %constant.108) | copy-start | bytes 3076
  14.1 71.3 %copy-start.8 = (bf16[1024,128]{1,0:T(8,128)(2,1)S(1)}, bf16[1024,128]{1,0:T(8,128)(2,1)}, u32[]{:S(2)}) copy-start(bf16[1024,128]{1,0:T(8,128)(2,1)} %param.19) | copy-start | bytes 786436
  14.1 71.3 %copy-start.9 = (bf16[1024,128]{1,0:T(8,128)(2,1)S(1)}, bf16[1024,128]{1,0:T(8,128)(2,1)}, u32[]{:S(2)}) copy-start(bf16[1024,128]{1,0:T(8,128)(2,1)} %param.18) | copy-start | bytes 786436
  38.6 300.6 %reduce-scatter.2.cloned.1.call-start = ((), (), s32[]{:S(2)}) async-start(), calls=%async_computation.4 | async-start | bytes 18939904 | tf_op jit(solution)/shard_map/reduce_scatter | solution.py:208
  140.6 1.9 copy-start.4
  140.6 2.3 copy-start.3
  144.1 4.3 %copy-start.5 = (bf16[2048,128]{1,0:T(8,128)(2,1)S(1)}, bf16[2048,128]{1,0:T(8,128)(2,1)}, u32[]{:S(2)}) copy-start(bf16[2048,128]{1,0:T(8,128)(2,1)} %param.31) | copy-start | bytes 1572868
  148.4 3.0 copy-start.6
  148.4 3.0 copy-start.7
  163.6 6.0 %copy-start.2 = (bf16[2,2048,128]{2,1,0:T(8,128)(2,1)S(1)}, bf16[2,2048,128]{2,1,0:T(8,128)(2,1)}, u32[]{:S(2)}) copy-start(bf16[2,2048,128]{2,1,0:T(8,128)(2,1)} %param.29) | copy-start | bytes 3145732
  231.8 0.7 copy-start.10
  232.4 116.6 %copy-start.12 = (f32[48,2]{0,1:T(2,128)S(1)}, f32[48,2]{0,1:T(2,128)}, u32[]{:S(2)}) copy-start(f32[48,2]{0,1:T(2,128)} %param.27) | copy-start | bytes 1156
  341.6 22.3 %all-to-all-start.1 = ((bf16[32,5,2048]{2,1,0:T(8,128)(2,1)}), bf16[32,5,2048]{2,1,0:T(8,128)(2,1)S(1)}, u32[]{:S(2)}, u32[]{:S(2)}) async-start(bf16[32,5,2048]{2,1,0:T(8,128)(2,1)} %convert_element_type.248), calls=%async_computation.2 | async-start | bytes 2097152 | tf_op jit(solution)/shard_map/all_to_all | solution.py:217
  363.9 5.1 %copy-start.1 = (bf16[2,128,2048]{2,1,0:T(8,128)(2,1)S(1)}, bf16[2,128,2048]{2,1,0:T(8,128)(2,1)}, u32[]{:S(2)}) copy-start(bf16[2,128,2048]{2,1,0:T(8,128)(2,1)} %param.30) | copy-start | bytes 3145732
Sparse Core Ops, SparseCore 0:
  10.4 43.6 all-gather.7
  55.9 64.1 all-gather.5
  231.9 107.2 reduce-scatter.1
where the time goes:
time: 379 us; the launch traced here: 376 us
  waiting for transfers between devices  120 us (32%)
  local copies, waits for them, and re-layouts  67.1 us (18%)
  blocking collectives  64.4 us (17%)
  other arithmetic  55.6 us (15%)
  matrix products  38.9 us (10%)
  between operations  22.3 us (6%)
  starting transfers between devices  7.39 us (2%)
    reduce_scatter x1, waiting for transfers between devices, local(): lax.psum_scatter(jnp.concatenate([mixer_term, routed_term, shared_term],...  107 us
    concatenate x1, local copies, waits for them, and re-layouts, local(): jnp.concatenate([mixer_term, routed_term, shared_term], axis=1)  24.4 us
    all_gather x2, blocking collectives, carried_in(): lax.all_gather(part.astype(kind), axis)  23.5 us
    another operation x1, other arithmetic, local(): running = jnp.cumsum(decay, axis=1)  23.2 us
    all_to_all x1, blocking collectives, local(): lax.all_to_all(outgoing, EP, split_axis=0, concat_axis=0, tiled=True)  23.2 us
    unnamed x2, blocking collectives  17.7 us
    dot_general x1, matrix products, local(): jnp.einsum('cejpf,jfd->cejpd', routed_hidden, expert_down, preferred_elem...  15.5 us
    transpose x1, local copies, waits for them, and re-layouts, local(): jnp.einsum('cejpf,jfd->cejpd', routed_hidden, expert_down, preferred_elem...  13.8 us
  transfers between devices with their start and end apart: 4, of which 2 were waited for; matrix products, arithmetic and copies ran while one was open for 22% of the time, Pallas kernels for 0%

commit v1 on v0

v1 whole, which is shorter than its diff:
```python
import functools

import jax
import jax.numpy as jnp
import numpy as np
from jax import lax
from jax.experimental import pallas as pl
from jax.experimental.pallas import tpu as pltpu
from jax.sharding import Mesh
from jax.sharding import PartitionSpec as P

EP = ("y", "x")
TP = ("z", "c")
ALL = ("y", "x", "z", "c")
MESH = pl.DeviceIdType.MESH
F32 = jnp.float32
BF16 = jnp.bfloat16
epsilon = 1e-06
turn_base = 10000.0

D = 2048
NE = 16
NZ = 8
BLOCK = 128
CAP = 5
TM = 48
PAIR = 2 * CAP
ROWS = NE * PAIR
HALF = ROWS // 2
PAD = 16
RET = 32
CO, CM, CR0, CR1 = 0, 1, 2, 3


def dot(a, b, dims=None, precision=None):
    if dims is None:
        return jnp.dot(a, b, preferred_element_type=F32, precision=precision)
    return lax.dot_general(a, b, (dims, ((), ())), preferred_element_type=F32)


def silu(v):
    return v / (1.0 + jnp.exp(-v))


def constants():
    place = np.zeros((2, NE * PAD, 128), np.float32)
    comb = np.zeros((3, 2, 128, NE * RET), np.float32)
    select = np.zeros((ROWS, NE * PAD), np.float32)
    perm = np.zeros((NE * RET, 3 * ROWS), np.float32)
    for j in range(NE):
        for rel in range(2):
            for p in range(CAP):
                place[rel, j * PAD + rel * CAP + p, j * CAP + p] = 1
                for zi in range(3):
                    comb[zi, rel, j * CAP + p, j * RET + zi * PAIR + rel * CAP + p] = 1
        for r in range(PAIR):
            select[j * PAIR + r, j * PAD + r] = 1
            for zi in range(3):
                perm[j * RET + zi * PAIR + r, zi * ROWS + j * PAIR + r] = 1
    return [jnp.asarray(m, BF16) for m in (place, comb, select, perm)]


def kernel(
    q_ref, k_ref, v_ref, g_ref, decay_ref, ow_ref, normed_ref, meta_ref,
    eg_ref, eu_ref, ed_ref, sg_ref, su_ref, sd_ref,
    cplace_ref, ccomb_ref, cselect_ref, cperm_ref,
    mixer_ref, channel_ref,
    wr, wd, ws, wsd, pn, pm, outg, a2a, ag_o, ag_m, ag_r, hid, ret_s, ret_r,
    acc, oth, othp, mix, mixp, rs_s, rs_r, rm_s, rm_r,
    st_s, st_r, before, state, entry, run_s, off_s,
    load_sem, w_s, w_r, pair_s, pair_r, a2a_s, a2a_r, ag_s, ag_v, st_ss, st_rs,
    ret_ss, ret_rs, oth_s, oth_r, mixp_s, mixp_r, rs_ss, rs_rs, rm_ss, rm_rs,
):
    y, x, z, c = (lax.axis_index(a) for a in ALL)
    me = y * 4 + x
    pc = 1 - c
    zup, zdown = lax.rem(z + 1, NZ), lax.rem(z + NZ - 1, NZ)
    partner = {"c": pc}

    def zat(offset):
        return lax.rem(z + (offset + NZ), NZ)

    def peer(j):
        return {"y": lax.div(j, 4), "x": lax.rem(j, 4)}

    def rcopy(src, dst, ss, rs, dev):
        return pltpu.make_async_remote_copy(
            src_ref=src, dst_ref=dst, send_sem=ss, recv_sem=rs, device_id=dev, device_id_type=MESH
        )

    barrier = pltpu.get_barrier_semaphore()
    for k in range(1, NE):
        pl.semaphore_signal(
            barrier, inc=1, device_id=peer(lax.rem(me + k, NE)), device_id_type=MESH
        )
    for dev in ({"z": zup}, {"z": zdown}, partner):
        pl.semaphore_signal(barrier, inc=1, device_id=dev, device_id_type=MESH)
    pl.semaphore_wait(barrier, NE + 2)

    pair = [
        rcopy(normed_ref, pn, pair_s.at[0], pair_r.at[0], partner),
        rcopy(meta_ref.at[pc], pm.at[0], pair_s.at[1], pair_r.at[1], partner),
        rcopy(meta_ref.at[2 + pc], pm.at[1], pair_s.at[2], pair_r.at[2], partner),
    ]
    for copy in pair:
        copy.start()

    def ag_copy(way, hop, chunk, src_z, first=False):
        buf = {CO: ag_o.at[src_z], CM: ag_m.at[src_z]}.get(chunk)
        if buf is None:
            buf = ag_r.at[src_z, chunk - CR0]
        src = normed_ref if first and chunk == CO else buf
        dev = {"z": zup if way == 0 else zdown}
        return rcopy(src, buf, ag_s.at[way, hop, chunk], ag_v.at[way, hop, chunk], dev)

    def ag_start(way, hop, chunk):
        ag_copy(way, hop, chunk, zat(-hop if way == 0 else hop)).start()

    def ag_wait(way, hop, chunk):
        ag_copy(way, hop, chunk, zat(-(hop + 1) if way == 0 else hop + 1)).wait_recv()

    for way in (0, 1):
        ag_copy(way, 0, CO, z, first=True).start()
    weights = [
        (eg_ref.at[pc], wr.at[1, :, pl.ds(0, 128)]),
        (eu_ref.at[pc], wr.at[1, :, pl.ds(128, 128)]),
        (ed_ref.at[pc], wd.at[pl.ds(128, 128)]),
        (sg_ref, ws.at[1, :, pl.ds(0, 128)]),
        (su_ref, ws.at[1, :, pl.ds(128, 128)]),
        (sd_ref, wsd.at[pl.ds(128, 128)]),
    ]
    sent = [rcopy(s, d, w_s.at[n], w_r.at[n], partner) for n, (s, d) in enumerate(weights)]
    loads = [
        (eg_ref.at[c], wr.at[0, :, pl.ds(0, 128)]),
        (eu_ref.at[c], wr.at[0, :, pl.ds(128, 128)]),
        (ed_ref.at[c], wd.at[pl.ds(0, 128)]),
        (sg_ref, ws.at[0, :, pl.ds(0, 128)]),
        (su_ref, ws.at[0, :, pl.ds(128, 128)]),
        (sd_ref, wsd.at[pl.ds(0, 128)]),
    ]
    loaded = [pltpu.make_async_copy(s, d, load_sem.at[n]) for n, (s, d) in enumerate(loads)]
    for copy in sent + loaded:
        copy.start()
    ag_o[z] = normed_ref[...]
    ag_m[z, pl.ds(0, TM)] = meta_ref[2 + c]
    for copy in pair:
        copy.wait_recv()
    ag_m[z, pl.ds(TM, TM)] = pm[1]
    for way in (0, 1):
        ag_start(way, 0, CM)

    def wide(count, body):
        def step(n, carry):
            body(pl.ds(pl.multiple_of(n * (D // count), D // count), D // count))
            return carry

        lax.fori_loop(0, count, step, 0)

    own_pick = dot(cplace_ref[0], meta_ref[c], ((1,), (1,))).astype(BF16)
    other_pick = dot(cplace_ref[1], pm[0], ((1,), (1,))).astype(BF16)

    def gather_rows(cols):
        rows = dot(own_pick, normed_ref[:, cols]) + dot(other_pick, pn[:, cols])
        outg[:, :, cols] = rows.astype(BF16).reshape(NE, PAD, D // 4)

    wide(4, gather_rows)

    def a2a_copy(j, slot):
        return rcopy(outg.at[j], a2a.at[slot], a2a_s.at[j], a2a_r.at[slot], peer(j))

    def over_peers(body):
        def step(k, carry):
            body(lax.rem(me + k, NE))
            return carry

        lax.fori_loop(1, NE, step, 0)

    over_peers(lambda j: a2a_copy(j, me).start())
    a2a[me] = outg[me]

    rows_i = lax.broadcasted_iota(jnp.int32, (BLOCK, BLOCK), 0)
    cols_i = lax.broadcasted_iota(jnp.int32, (BLOCK, BLOCK), 1)
    upper = (rows_i <= cols_i).astype(F32)
    lower = rows_i >= cols_i
    run_s[...] = dot(decay_ref[...], upper, precision=lax.Precision.HIGHEST)
    state[...] = jnp.zeros_like(state)

    def along(row):
        return jnp.transpose(jnp.broadcast_to(row, (BLOCK, BLOCK)))

    def local_state(n, total):
        rows = pl.ds(pl.multiple_of(n * BLOCK, BLOCK), BLOCK)
        row = run_s[pl.ds(n, 1), :]
        end = row[:, BLOCK - 1 :]
        off_s[pl.ds(n, 1), :] = jnp.broadcast_to(total, (1, BLOCK))
        tail = jnp.exp(end - along(row))
        keyed = (k_ref[rows, :].astype(F32) * tail).astype(BF16)
        before[n] = state[...]
        state[...] = jnp.exp(end) * state[...] + dot(keyed, v_ref[rows, :], ((0,), (0,)))
        return total + end

    total = lax.fori_loop(0, NZ, local_state, jnp.zeros((1, 1), F32))
    st_s[pl.ds(0, BLOCK), :] = state[...].astype(BF16)
    high = total.astype(BF16).astype(F32)
    middle = (total - high).astype(BF16).astype(F32)
    low = total - high - middle
    line = lax.broadcasted_iota(jnp.int32, (16, 256), 0)
    pieces = jnp.where(line == 0, high, jnp.where(line == 1, middle, jnp.where(line == 2, low, 0.0)))
    st_s[pl.ds(BLOCK, 16), :] = pieces.astype(BF16)

    def st_copy(j, slot):
        return rcopy(st_s, st_r.at[slot], st_ss.at[j], st_rs.at[slot], peer(j))

    def each_later(body):
        def step(j, carry):
            @pl.when(j > me)
            def _():
                body(j)

            return carry

        lax.fori_loop(1, NE, step, 0)

    each_later(lambda j: st_copy(j, me).start())

    over_peers(lambda j: a2a_copy(j, j).wait_recv())

    def pack_rows(cols):
        rows = dot(cselect_ref[...], a2a[:, :, cols].reshape(NE * PAD, D // 4))
        ag_r[z, :, :, cols] = rows.astype(BF16).reshape(2, HALF, D // 4)

    wide(4, pack_rows)
    for chunk in (CR0, CR1):
        for way in (0, 1):
            ag_start(way, 0, chunk)
    for chunk in (CO, CM):
        for way in (0, 1):
            ag_wait(way, 0, chunk)
            ag_start(way, 1, chunk)
    for copy in loaded:
        copy.wait()
    for copy in sent:
        copy.wait_recv()

    def hidden(rows, weight):
        parts = []
        for n in (0, 1):
            both = dot(rows, weight[n])
            parts.append((silu(both[:, :128]) * both[:, 128:]).astype(BF16))
        return jnp.concatenate(parts, axis=1)

    def shared(za, zb=None):
        rows = ag_o[za] if zb is None else jnp.concatenate([ag_o[za], ag_o[zb]], axis=0)
        h = hidden(rows, ws)

        def down(cols):
            result = dot(h, wsd[:, cols])
            acc[za, :, cols] = result[:TM]
            if zb is not None:
                acc[zb, :, cols] = result[TM:]

        wide(4, down)

    hid[2] = hidden(ag_r[z].reshape(ROWS, D), wr)
    shared(z)

    entry[...] = jnp.zeros_like(entry)

    def take_state(j, carry):
        @pl.when(j < me)
        def _():
            st_copy(j, j).wait_recv()
            sums = st_r[j, pl.ds(BLOCK, 16), :].astype(F32)
            decay = jnp.exp(sums[0:1] + sums[1:2] + sums[2:3])
            entry[...] = decay * entry[...] + st_r[j, pl.ds(0, BLOCK), :].astype(F32)

        return carry

    lax.fori_loop(0, NE - 1, take_state, 0)

    def retain(n, carry):
        rows = pl.ds(pl.multiple_of(n * BLOCK, BLOCK), BLOCK)
        row = run_s[pl.ds(n, 1), :]
        spread = along(row)
        query, key, value = q_ref[rows, :], k_ref[rows, :], v_ref[rows, :]
        scores = dot(query, key, ((1,), (1,)))
        factor = jnp.exp(jnp.where(lower, spread - row, 0.0))
        mixed = jnp.where(lower, scores * factor, 0.0).astype(BF16)
        scaled_query = (query.astype(F32) * jnp.exp(spread)).astype(BF16)
        offset = jnp.exp(off_s[pl.ds(n, 1), :][:, 0:1])
        prior = (before[n] + offset * entry[...]).astype(BF16)
        kept = dot(mixed, value) + dot(scaled_query, prior)
        scale = lax.rsqrt(jnp.mean(kept * kept, axis=-1, keepdims=True) + epsilon)
        gated = (silu(g_ref[rows, :].astype(F32)) * (kept * scale)).astype(BF16)

        def project(cols):
            term = dot(gated, ow_ref[:, cols]).astype(BF16)
            mix[0, n, :, cols] = term[:64]
            mix[1, n, :, cols] = term[64:]

        wide(4, project)
        return carry

    lax.fori_loop(0, NZ, retain, 0)
    mix_copy = rcopy(mix.at[pc], mixp, mixp_s, mixp_r, partner)
    mix_copy.start()

    def ret_copy(g, j, slot):
        return rcopy(
            ret_s.at[g, j], ret_r.at[g, slot], ret_ss.at[g, j], ret_rs.at[g, slot], peer(j)
        )

    def far(hop, chunk):
        if chunk in (CO, CR0):
            ag_start(0, hop, chunk)
        else:
            ag_start(1, hop, chunk)

    def hop_step(h, carry):
        za, zb = zat(-h), zat(h)
        for k in (0, 1):
            for way in (0, 1):
                ag_wait(way, h - 1, CR0 + k)

            @pl.when(h < 3)
            def _():
                for way in (0, 1):
                    ag_start(way, h, CR0 + k)

            @pl.when(h == 3)
            def _():
                far(3, CR0 + k)

            if k == 0:

                @pl.when(h > 1)
                def _():
                    for chunk in (CO, CM):
                        for way in (0, 1):
                            ag_wait(way, h - 1, chunk)

                @pl.when(h == 2)
                def _():
                    for chunk in (CO, CM):
                        for way in (0, 1):
                            ag_start(way, 2, chunk)

                @pl.when(h == 3)
                def _():
                    for chunk in (CO, CM):
                        far(3, chunk)

            h_rows = hidden(jnp.concatenate([ag_r[za, k], ag_r[zb, k]], axis=0), wr)
            hid[0, pl.ds(k * HALF, HALF)] = h_rows[:HALF]
            hid[1, pl.ds(k * HALF, HALF)] = h_rows[HALF:]
        shared(za, zb)

        @pl.when(h == 3)
        def _():
            ag_wait(0, 3, CR0)
            ag_wait(1, 3, CR1)
            ag_wait(0, 3, CO)
            ag_wait(1, 3, CM)
            hid[2] = hidden(ag_r[zat(4)].reshape(ROWS, D), wr)
            shared(zat(4))

        g = h - 1
        placed = dot(cperm_ref[...], hid[...].reshape(3 * ROWS, 256)).astype(BF16)

        def down(cols):
            result = dot(placed, wd[:, cols]).astype(BF16)
            ret_s[g, :, :, cols] = result.reshape(NE, RET, D // 8)

        wide(8, down)
        over_peers(lambda j: ret_copy(g, j, me).start())
        ret_r[g, me] = ret_s[g, me]
        return carry

    lax.fori_loop(1, 4, hop_step, 0)

    def chain(base, send, recv, ss, rs, rows):
        def copy(way, s):
            dev = {"z": zup if way == 0 else zdown}
            src, dst = send.at[way, s], recv.at[way, s]
            if s == 0:
                cols = pl.ds(way * (D // 2), D // 2)
                src, dst = src.at[:, cols], dst.at[:, cols]
            return rcopy(src, dst, ss.at[way, s], rs.at[way, s], dev)

        def step(s):
            for way in (0, 1):
                target = zat(4 - s if way == 0 else s - 4)
                if s == 0:
                    cols = pl.ds(way * (D // 2), D // 2)
                    send[way, s, :, cols] = base(target, cols).astype(BF16)
                else:
                    copy(way, s - 1).wait_recv()
                    for part in (0, 1):
                        cols = pl.ds(part * (D // 2), D // 2)
                        value = base(target, cols)
                        if s > 1 or part == way:
                            value = value + recv[way, s - 1, :, cols].astype(F32)
                        send[way, s, :, cols] = value.astype(BF16)
                copy(way, s).start()

        def finish(out_ref):
            for way in (0, 1):
                copy(way, 3).wait_recv()
            for part in (0, 1):
                cols = pl.ds(part * (D // 2), D // 2)
                value = base(z, cols)
                for way in (0, 1):
                    value = value + recv[way, 3, :, cols].astype(F32)
                out_ref[:, cols] = value.astype(BF16)

        def drain():
            for way in (0, 1):
                for s in range(4):
                    copy(way, s).wait_send()

        return step, finish, drain

    def mix_base(target, cols):
        return mix[c, target, :, cols].astype(F32) + mixp[target, :, cols].astype(F32)

    def moe_base(target, cols):
        return acc[target, :, cols] + othp[target, :, cols].astype(F32)

    mix_step, mix_finish, mix_drain = chain(mix_base, rm_s, rm_r, rm_ss, rm_rs, 64)
    moe_step, moe_finish, moe_drain = chain(moe_base, rs_s, rs_r, rs_ss, rs_rs, TM)

    sources = [(0, 0, -1), (0, 1, 1), (0, 2, 0), (1, 0, -2), (1, 1, 2), (2, 0, -3), (2, 1, 3), (2, 2, 4)]

    def oth_copy(n):
        where = zat(sources[n][2])
        return rcopy(oth.at[where], othp.at[where], oth_s.at[n], oth_r.at[n], partner)

    def combine(g):
        over_peers(lambda j: ret_copy(g, j, j).wait_recv())
        for n, (group, zi, offset) in enumerate(sources):
            if group != g:
                continue
            where = zat(offset)
            weight = ag_m[where]
            spread = jnp.concatenate(
                [dot(weight[:TM], ccomb_ref[zi, 0]), dot(weight[TM:], ccomb_ref[zi, 1])], axis=0
            ).astype(BF16)

            def gather(cols):
                result = dot(spread, ret_r[g, :, :, cols].reshape(NE * RET, D // 4))
                acc[where, :, cols] += result[:TM]
                oth[where, :, cols] = result[TM:].astype(BF16)

            wide(4, gather)
            oth_copy(n).start()

    mix_copy.wait_recv()
    mix_step(0)
    combine(0)
    mix_step(1)
    combine(1)
    mix_step(2)
    mix_step(3)
    combine(2)
    for n in range(NZ):
        oth_copy(n).wait_recv()
    moe_step(0)
    mix_finish(mixer_ref)
    for s in (1, 2, 3):
        moe_step(s)
    moe_finish(channel_ref)

    for copy in pair + sent + [mix_copy]:
        copy.wait_send()
    over_peers(lambda j: a2a_copy(j, me).wait_send())
    each_later(lambda j: st_copy(j, me).wait_send())
    for way in (0, 1):
        ag_copy(way, 0, CO, z, first=True).wait_send()
        for hop in range(3):
            for chunk in (CO, CM, CR0, CR1):
                if hop or chunk != CO:
                    ag_copy(way, hop, chunk, z).wait_send()
    for way, chunk in ((0, CO), (1, CM), (0, CR0), (1, CR1)):
        ag_copy(way, 3, chunk, z).wait_send()
    for g in range(3):
        over_peers(lambda j: ret_copy(g, j, me).wait_send())
    for n in range(NZ):
        oth_copy(n).wait_send()
    mix_drain()
    moe_drain()


def fused(*args):
    vmem = pl.BlockSpec(memory_space=pltpu.VMEM)
    hbm = pl.BlockSpec(memory_space=pl.ANY)
    sem = pltpu.SemaphoreType.DMA
    scratch = [
        pltpu.VMEM(s, t)
        for s, t in (
            ((2, D, 256), BF16), ((256, D), BF16), ((2, D, 256), BF16), ((256, D), BF16),
            ((TM, D), BF16), ((2, TM, 128), BF16),
            ((NE, PAD, D), BF16), ((NE, PAD, D), BF16),
            ((NZ, TM, D), BF16), ((NZ, 2 * TM, 128), BF16), ((NZ, 2, HALF, D), BF16),
            ((3, ROWS, 256), BF16),
            ((3, NE, RET, D), BF16), ((3, NE, RET, D), BF16),
            ((NZ, TM, D), F32), ((NZ, TM, D), BF16), ((NZ, TM, D), BF16),
            ((2, NZ, 64, D), BF16), ((NZ, 64, D), BF16),
            ((2, 4, TM, D), BF16), ((2, 4, TM, D), BF16),
            ((2, 4, 64, D), BF16), ((2, 4, 64, D), BF16),
            ((144, 256), BF16), ((NE, 144, 256), BF16),
            ((NZ, BLOCK, 256), F32), ((BLOCK, 256), F32), ((BLOCK, 256), F32),
            ((NZ, BLOCK), F32), ((NZ, BLOCK), F32),
        )
    ] + [
        sem((6,)), sem((6,)), sem((6,)), sem((3,)), sem((3,)), sem((NE,)), sem((NE,)),
        sem((2, 4, 4)), sem((2, 4, 4)), sem((NE,)), sem((NE,)),
        sem((3, NE)), sem((3, NE)), sem((NZ,)), sem((NZ,)), sem, sem,
        sem((2, 4)), sem((2, 4)), sem((2, 4)), sem((2, 4)),
    ]
    return pl.pallas_call(
        kernel,
        out_shape=(jax.ShapeDtypeStruct((64, D), BF16), jax.ShapeDtypeStruct((TM, D), BF16)),
        in_specs=[vmem] * 8 + [hbm] * 6 + [vmem] * 4,
        out_specs=(vmem, vmem),
        scratch_shapes=scratch,
        compiler_params=pltpu.CompilerParams(
            collective_id=0, has_side_effects=True, vmem_limit_bytes=67043328
        ),
    )(*args)


def turn(rows, position):
    half = rows.shape[-1] // 2
    inverse = turn_base ** (-jnp.arange(half, dtype=F32) / half)
    angles = position[:, None] * inverse[None, :]
    cosine, sine = jnp.cos(angles), jnp.sin(angles)
    wide = rows.astype(F32)
    first, second = wide[:, :half], wide[:, half:]
    return jnp.concatenate(
        [first * cosine - second * sine, second * cosine + first * sine], axis=-1
    ).astype(BF16)


def routing(routes, route_weight, expert_count):
    flat = routes.reshape(-1)
    onehot = (flat[:, None] == jnp.arange(expert_count, dtype=jnp.int32)[None, :]).astype(BF16)
    count = flat.shape[0]
    strict = jnp.asarray(np.tril(np.ones((count, count), np.float32), -1), BF16)
    earlier = jnp.dot(strict, onehot, preferred_element_type=F32)
    rank = jnp.sum(earlier * onehot.astype(F32), axis=1).astype(jnp.int32).reshape(routes.shape)
    lane = (routes // 2) * CAP + rank
    hit = (lane[:, :, None] == jnp.arange(128, dtype=jnp.int32)).astype(F32)
    parity = (routes[:, :, None] % 2) == jnp.arange(2, dtype=jnp.int32)
    share = parity.astype(F32)
    place = jnp.einsum("nkl,nke->enl", hit, share)
    comb = jnp.einsum("nkl,nke->enl", hit * route_weight[:, :, None], share)
    return jnp.concatenate([place, comb], axis=0).astype(BF16)


def local(
    query_rows, key_rows, value_rows, gate_rows, log_decay, out_weight, channel_input, norm_gain,
    routes, route_weight, expert_gate, expert_up, expert_down, shared_gate, shared_up, shared_down,
):
    tokens = query_rows.shape[0]
    position = (lax.axis_index(EP) * tokens + jnp.arange(tokens, dtype=jnp.int32)).astype(F32)
    queries = turn(query_rows, position)
    keys = turn(key_rows, position)
    wide = channel_input.astype(F32)
    normed = (
        wide * lax.rsqrt(jnp.mean(wide * wide, axis=-1, keepdims=True) + epsilon) * norm_gain
    ).astype(BF16)
    meta = routing(routes, route_weight, 2 * NE)
    return fused(
        queries, keys, value_rows, gate_rows, log_decay.reshape(NZ, BLOCK), out_weight, normed,
        meta, expert_gate, expert_up, expert_down, shared_gate, shared_up, shared_down,
        *constants(),
    )


def solution(mesh):
    split = Mesh(mesh.devices.reshape(4, 4, NZ, 2), ALL)
    return jax.shard_map(
        local,
        mesh=split,
        in_specs=(
            P(EP, TP), P(EP, TP), P(EP, TP), P(EP, TP), P(TP, EP), P(TP, None),
            P(ALL, None), P(), P(ALL, None), P(ALL, None),
            P(EP, None, TP), P(EP, None, TP), P(EP, TP, None),
            P(None, TP), P(None, TP), P(TP, None),
        ),
        out_specs=(P(ALL, None), P(ALL, None)),
        check_vma=False,
    )
```

time: 379 us -> 187 us (0.49)
  the two profiles are of different devices: /device:TPU:2 before, /device:TPU:24 now
where the time goes in v1:
time: 187 us; the launch traced here: 186 us
  Pallas kernels  174 us (93%)
  other arithmetic  6.31 us (3%)
  local copies, waits for them, and re-layouts  4.43 us (2%)
    pallas_call x1, Pallas kernels, fused(): pl.pallas_call(kernel, out_shape=(jax.ShapeDtypeStruct((64, D), BF16), ja...  174 us
    unnamed x18, local copies, waits for them, and re-layouts  4.07 us

profile of v1, /device:TPU:24, one launch (start us, length us, event | category | flops | bytes accessed | tf_op | source)
XLA Modules:
  0.0 186.4 jit_solution(975567330293910698)
XLA Ops:
  0.6 0.0 copy-start.1
  0.6 1.0 convert_element_type.39
  1.7 0.0 copy-done.1
  1.8 2.5 %fusion.14 = (bf16[1024,64]{1,0:T(8,128)(2,1)S(1)}, bf16[1024,64]{1,0:T(8,128)(2,1)S(1)}, bf16[1024,64]{1,0:T(8,128)(2,1)S(1)}, bf16[1024,64]{1,0:T(8,128)(2,1)S(1)}) fusion(f32[1024,128]{1,0:T(8,128)S(1)} %convert_element_type.39, f32[1024]{0:T(1024)S(1)} %add_convert_fusion, f32[64]{0:T(128)S(1)} %multiply_power_fusion, ...), kind=kLoop, calls=%fused_computation.17 | loop fusion | flops 1114112 | bytes 1577216 | tf_op jit(solution)/shard_map/convert.4
  4.3 0.0 copy-start
  4.3 1.1 pad_maximum_fusion
  5.4 0.0 copy-done
  5.4 0.0 copy-start.3
  5.4 0.1 fusion.17
  5.6 0.5 copy-done.3
  6.1 0.0 copy-start.4
  6.1 0.8 fusion.19.normed_ref
  6.9 0.0 copy-done.4
  6.9 0.1 copy.50
  7.0 0.0 copy-start.6
  7.0 0.1 copy.47
  7.1 0.1 eq.46
  7.2 0.5 copy-done.6
  7.8 0.1 fusion
  7.9 0.1 convert_element_type.45
  8.1 0.0 copy-start.5
  8.1 0.3 fusion.21
  8.4 0.4 copy-done.5
  8.8 0.1 copy.55
  8.9 0.3 fusion.22
  9.2 0.6 pad_maximum_fusion.2.meta_ref
  9.8 174.2 %shard_map.212 = (bf16[64,2048]{1,0:T(8,128)(2,1)}, bf16[48,2048]{1,0:T(8,128)(2,1)}) custom-call(bf16[1024,128]{1,0:T(8,128)(2,1)} %get-tuple-element.10.q_ref, bf16[1024,128]{1,0:T(8,128)(2,1)} %get-tuple-element.11.k_ref, bf16[1024,256]{1,0:T(8,128)(2,1)} %v_ref.1, bf16[1024,256]{1,0:T(8,128)(2,1)} %g_ref.1, f32[8,128]{1,0:T(8,128)} %bitcast.6, ...), custom_call_target="tpu_custom_call" | custom-call | tf_op jit(solution)/shard_map/pallas_call | solution.py:520
  184.0 0.0 copy-start.2
  184.0 1.7 copy.65
  185.7 0.0 copy-done.2
  185.7 0.7 copy.66
  (8 shorter events, 0.1 us)
Async XLA Ops:
  0.6 1.1 copy-start.1
  4.3 1.1 copy-start
  5.4 0.7 copy-start.3
  6.1 0.8 copy-start.4
  7.0 0.7 copy-start.6
  8.1 0.7 copy-start.5
  184.0 1.7 copy-start.2

commit v2 on v1

v2 whole, which is shorter than its diff:
```python
import functools

import jax
import jax.numpy as jnp
import numpy as np
from jax import lax
from jax.experimental import pallas as pl
from jax.experimental.pallas import tpu as pltpu
from jax.sharding import Mesh
from jax.sharding import PartitionSpec as P

EP = ("y", "x")
TP = ("z", "c")
ALL = ("y", "x", "z", "c")
MESH = pl.DeviceIdType.MESH
F32 = jnp.float32
BF16 = jnp.bfloat16
epsilon = 1e-06
turn_base = 10000.0

D = 2048
NE = 16
NZ = 8
BLOCK = 128
CAP = 5
TM = 48
PAIR = 2 * CAP
ROWS = NE * PAIR
HALF = ROWS // 2
PAD = 16
RET = 32
CO, CM, CR0, CR1 = 0, 1, 2, 3
SENT = (16, 24, 24, 32)
ORDER = (
    (2, 2), (3, 2), (2, 3), (1, 2), (2, 1), (2, 0), (0, 2), (3, 1), (1, 3), (3, 3), (1, 1),
    (3, 0), (0, 3), (1, 0), (0, 1),
)


def dot(a, b, dims=None, precision=None):
    if dims is None:
        return jnp.dot(a, b, preferred_element_type=F32, precision=precision)
    return lax.dot_general(a, b, (dims, ((), ())), preferred_element_type=F32)


def silu(v):
    return v / (1.0 + jnp.exp(-v))


def constants():
    place = np.zeros((2, NE * PAD, 128), np.float32)
    comb = np.zeros((3, 2, 128, NE * RET), np.float32)
    comb_own = np.zeros((2, 128, NE * PAD), np.float32)
    select = np.zeros((ROWS, NE * PAD), np.float32)
    perm = np.zeros((NE * RET, 3 * ROWS), np.float32)
    for j in range(NE):
        for rel in range(2):
            for p in range(CAP):
                comb_own[rel, j * CAP + p, j * PAD + rel * CAP + p] = 1
                place[rel, j * PAD + rel * CAP + p, j * CAP + p] = 1
                for zi in range(3):
                    comb[zi, rel, j * CAP + p, j * RET + zi * PAIR + rel * CAP + p] = 1
        for r in range(PAIR):
            select[j * PAIR + r, j * PAD + r] = 1
            for zi in range(3):
                perm[j * RET + zi * PAIR + r, zi * ROWS + j * PAIR + r] = 1
    rate = turn_base ** (-(np.arange(128) % 64) / 64.0)
    near = np.arange(BLOCK)[:, None] * rate
    far = np.arange(128)[:, None] * float(BLOCK) * rate
    turns = np.stack([np.cos(near), np.sin(near), np.cos(far), np.sin(far)])
    tables = [jnp.asarray(m, BF16) for m in (place, comb, comb_own, select, perm)]
    return tables + [jnp.asarray(turns, F32)]


def kernel(
    chan_ref, gain_ref, routes_ref, share_ref,
    q_hbm, k_hbm, v_hbm, g_hbm, decay_hbm, ow_hbm,
    eg_ref, eu_ref, ed_ref, sg_ref, su_ref, sd_ref,
    cplace_hbm, ccomb_hbm, ccomb0_hbm, cselect_hbm, cperm_hbm, turns_hbm,
    mixer_ref, channel_ref,
    q_ref, k_ref, v_ref, g_ref, decay_ref, ow_ref,
    cplace_ref, ccomb_ref, ccomb0_ref, cselect_ref, cperm_ref, turns_ref, normed_ref, meta_ref, keys,
    wr, wd, ws, wsd, pn, pm, outg, a2a, ag_o, ag_m, ag_r, hid, ret_s, ret_r,
    acc, oth, othp, mix, mixp, rs_s, rs_r, rm_s, rm_r,
    st_s, st_r, before, state, entry, run_s, off_s,
    in_sem, load_sem, w_s, w_r, pair_s, pair_r, a2a_s, a2a_r, ag_s, ag_v, st_ss, st_rs,
    ret_ss, ret_rs, oth_s, oth_r, mixp_s, mixp_r, rs_ss, rs_rs, rm_ss, rm_rs,
):
    y, x, z, c = (lax.axis_index(a) for a in ALL)
    me = y * 4 + x
    pc = 1 - c
    zup, zdown = lax.rem(z + 1, NZ), lax.rem(z + NZ - 1, NZ)
    partner = {"c": pc}

    def zat(offset):
        return lax.rem(z + (offset + NZ), NZ)

    def peer(j):
        return {"y": lax.div(j, 4), "x": lax.rem(j, 4)}

    others = [lax.rem(y + dy, 4) * 4 + lax.rem(x + dx, 4) for dy, dx in ORDER]

    def over_peers(body):
        for j in others:
            body(j)

    def rcopy(src, dst, ss, rs, dev):
        return pltpu.make_async_remote_copy(
            src_ref=src, dst_ref=dst, send_sem=ss, recv_sem=rs, device_id=dev, device_id_type=MESH
        )

    for g in (1, 2):
        ret_r[g, :, pl.ds(16, 16), :] = jnp.zeros((NE, 16, D), BF16)
    barrier = pltpu.get_barrier_semaphore()
    for j in others:
        pl.semaphore_signal(barrier, inc=1, device_id=peer(j), device_id_type=MESH)
    for dev in ({"z": zup}, {"z": zdown}, partner):
        pl.semaphore_signal(barrier, inc=1, device_id=dev, device_id_type=MESH)
    incoming = [
        (cplace_hbm, cplace_ref), (k_hbm, k_ref), (v_hbm, v_ref), (decay_hbm, decay_ref),
        (turns_hbm, turns_ref), (cselect_hbm, cselect_ref), (q_hbm, q_ref), (g_hbm, g_ref),
        (ow_hbm, ow_ref), (cperm_hbm, cperm_ref), (ccomb0_hbm, ccomb0_ref), (ccomb_hbm, ccomb_ref),
    ]
    arriving = [pltpu.make_async_copy(s, d, in_sem.at[n]) for n, (s, d) in enumerate(incoming)]
    for copy in arriving:
        copy.start()

    wide_rows = chan_ref[...].astype(F32)
    mean = jnp.mean(wide_rows * wide_rows, axis=-1, keepdims=True)
    normed_ref[...] = (wide_rows * lax.rsqrt(mean + epsilon) * gain_ref[...]).astype(BF16)
    lanes = lax.broadcasted_iota(jnp.int32, (TM, 128), 1)
    picks = [routes_ref[:, k : k + 1] for k in (0, 1)]
    hits = [(lanes == pick).astype(F32) for pick in picks]
    strict = lax.broadcasted_iota(jnp.int32, (TM, TM), 0) > lax.broadcasted_iota(
        jnp.int32, (TM, TM), 1
    )
    earlier = dot(strict.astype(F32).astype(BF16), (hits[0] + hits[1]).astype(BF16))
    metas = [jnp.zeros((TM, 128), F32)] * 4
    for k in (0, 1):
        rank = jnp.sum(earlier * hits[k], axis=-1, keepdims=True)
        slot = (picks[k] >> 1).astype(F32) * CAP + rank
        there = (lanes.astype(F32) == slot).astype(F32)
        for parity in (0, 1):
            mine = there * ((picks[k] & 1) == parity).astype(F32)
            metas[parity] += mine
            metas[2 + parity] += mine * share_ref[:, k : k + 1]
    for n in range(4):
        meta_ref[n] = metas[n].astype(BF16)
    pl.semaphore_wait(barrier, NE + 2)

    pair = [
        rcopy(normed_ref, pn, pair_s.at[0], pair_r.at[0], partner),
        rcopy(meta_ref.at[pc], pm.at[0], pair_s.at[1], pair_r.at[1], partner),
        rcopy(meta_ref.at[2 + pc], pm.at[1], pair_s.at[2], pair_r.at[2], partner),
    ]
    for copy in pair:
        copy.start()

    def ag_copy(way, hop, chunk, src_z, first=False):
        buf = {CO: ag_o.at[src_z], CM: ag_m.at[src_z]}.get(chunk)
        if buf is None:
            buf = ag_r.at[src_z, chunk - CR0]
        src = normed_ref if first and chunk == CO else buf
        dev = {"z": zup if way == 0 else zdown}
        return rcopy(src, buf, ag_s.at[way, hop, chunk], ag_v.at[way, hop, chunk], dev)

    def ag_start(way, hop, chunk):
        ag_copy(way, hop, chunk, zat(-hop if way == 0 else hop)).start()

    def ag_wait(way, hop, chunk):
        ag_copy(way, hop, chunk, zat(-(hop + 1) if way == 0 else hop + 1)).wait_recv()

    for way in (0, 1):
        ag_copy(way, 0, CO, z, first=True).start()
    weights = [
        (eg_ref.at[pc], wr.at[1, :, pl.ds(0, 128)]),
        (eu_ref.at[pc], wr.at[1, :, pl.ds(128, 128)]),
        (ed_ref.at[pc], wd.at[pl.ds(128, 128)]),
        (sg_ref, ws.at[1, :, pl.ds(0, 128)]),
        (su_ref, ws.at[1, :, pl.ds(128, 128)]),
        (sd_ref, wsd.at[pl.ds(128, 128)]),
    ]
    sent = [rcopy(s, d, w_s.at[n], w_r.at[n], partner) for n, (s, d) in enumerate(weights)]
    loads = [
        (eg_ref.at[c], wr.at[0, :, pl.ds(0, 128)]),
        (eu_ref.at[c], wr.at[0, :, pl.ds(128, 128)]),
        (ed_ref.at[c], wd.at[pl.ds(0, 128)]),
        (sg_ref, ws.at[0, :, pl.ds(0, 128)]),
        (su_ref, ws.at[0, :, pl.ds(128, 128)]),
        (sd_ref, wsd.at[pl.ds(0, 128)]),
    ]
    loaded = [pltpu.make_async_copy(s, d, load_sem.at[n]) for n, (s, d) in enumerate(loads)]
    for copy in sent + loaded:
        copy.start()
    ag_o[z] = normed_ref[...]
    ag_m[z, pl.ds(0, TM)] = meta_ref[2 + c]
    for copy in pair:
        copy.wait_recv()
    ag_m[z, pl.ds(TM, TM)] = pm[1]
    for way in (0, 1):
        ag_start(way, 0, CM)

    def wide(count, body):
        def step(n, carry):
            body(pl.ds(pl.multiple_of(n * (D // count), D // count), D // count))
            return carry

        lax.fori_loop(0, count, step, 0)

    arriving[0].wait()
    own_pick = dot(cplace_ref[0], meta_ref[c], ((1,), (1,))).astype(BF16)
    other_pick = dot(cplace_ref[1], pm[0], ((1,), (1,))).astype(BF16)

    def gather_rows(cols):
        rows = dot(own_pick, normed_ref[:, cols]) + dot(other_pick, pn[:, cols])
        outg[:, :, cols] = rows.astype(BF16).reshape(NE, PAD, D // 4)

    wide(4, gather_rows)

    def a2a_copy(j, slot):
        return rcopy(outg.at[j], a2a.at[slot], a2a_s.at[j], a2a_r.at[slot], peer(j))

    over_peers(lambda j: a2a_copy(j, me).start())
    a2a[me] = outg[me]

    def relay_own(hop):
        for chunk in (CO, CM):
            for way in (0, 1):
                ag_wait(way, hop, chunk)
        if hop < 2:
            for chunk in (CO, CM):
                for way in (0, 1):
                    ag_start(way, hop + 1, chunk)
        else:
            ag_start(0, 3, CO)
            ag_start(1, 3, CM)

    for copy in arriving[1:5]:
        copy.wait()
    half_lane = lax.broadcasted_iota(jnp.int32, (BLOCK, BLOCK), 1) < 64

    def turned(ref, n):
        rows = ref[pl.ds(pl.multiple_of(n * BLOCK, BLOCK), BLOCK), :].astype(F32)
        far_line = pl.ds(me * NZ + n, 1)
        near_cos, near_sin = turns_ref[0], turns_ref[1]
        far_cos, far_sin = turns_ref[2, far_line, :], turns_ref[3, far_line, :]
        cosine = far_cos * near_cos - far_sin * near_sin
        sine = far_sin * near_cos + far_cos * near_sin
        swapped = pltpu.roll(rows, 64, 1)
        return (rows * cosine + swapped * jnp.where(half_lane, -sine, sine)).astype(BF16)

    rows_i = lax.broadcasted_iota(jnp.int32, (BLOCK, BLOCK), 0)
    cols_i = lax.broadcasted_iota(jnp.int32, (BLOCK, BLOCK), 1)
    upper = (rows_i <= cols_i).astype(F32)
    lower = rows_i >= cols_i
    run_s[...] = dot(decay_ref[...], upper, precision=lax.Precision.HIGHEST)
    state[...] = jnp.zeros_like(state)

    def along(row):
        return jnp.transpose(jnp.broadcast_to(row, (BLOCK, BLOCK)))

    def local_state(n, total):
        rows = pl.ds(pl.multiple_of(n * BLOCK, BLOCK), BLOCK)
        row = run_s[pl.ds(n, 1), :]
        end = row[:, BLOCK - 1 :]
        off_s[pl.ds(n, 1), :] = jnp.broadcast_to(total, (1, BLOCK))
        tail = jnp.exp(end - along(row))
        key = turned(k_ref, n)
        keys[rows, :] = key
        keyed = (key.astype(F32) * tail).astype(BF16)
        before[n] = state[...]
        state[...] = jnp.exp(end) * state[...] + dot(keyed, v_ref[rows, :], ((0,), (0,)))
        return total + end

    total = lax.fori_loop(0, NZ, local_state, jnp.zeros((1, 1), F32))
    st_s[pl.ds(0, BLOCK), :] = state[...].astype(BF16)
    high = total.astype(BF16).astype(F32)
    middle = (total - high).astype(BF16).astype(F32)
    low = total - high - middle
    line = lax.broadcasted_iota(jnp.int32, (16, 256), 0)
    pieces = jnp.where(line == 0, high, jnp.where(line == 1, middle, jnp.where(line == 2, low, 0.0)))
    st_s[pl.ds(BLOCK, 16), :] = pieces.astype(BF16)

    def st_copy(j, slot):
        return rcopy(st_s, st_r.at[slot], st_ss.at[j], st_rs.at[slot], peer(j))

    def each_later(body):
        for j in others:

            @pl.when(j > me)
            def _():
                body(j)

    relay_own(0)
    relay_own(1)

    over_peers(lambda j: a2a_copy(j, j).wait_recv())
    each_later(lambda j: st_copy(j, me).start())
    arriving[5].wait()

    def pack_rows(cols):
        rows = dot(cselect_ref[...], a2a[:, :, cols].reshape(NE * PAD, D // 4))
        ag_r[z, :, :, cols] = rows.astype(BF16).reshape(2, HALF, D // 4)

    wide(4, pack_rows)
    for chunk in (CR0, CR1):
        for way in (0, 1):
            ag_start(way, 0, chunk)
    for copy in loaded + arriving[9:10]:
        copy.wait()
    for copy in sent:
        copy.wait_recv()

    def hidden(rows, weight):
        parts = []
        for n in (0, 1):
            both = dot(rows, weight[n])
            parts.append((silu(both[:, :128]) * both[:, 128:]).astype(BF16))
        return jnp.concatenate(parts, axis=1)

    def shared(za, zb=None):
        rows = ag_o[za] if zb is None else jnp.concatenate([ag_o[za], ag_o[zb]], axis=0)
        h = hidden(rows, ws)

        def down(cols):
            result = dot(h, wsd[:, cols])
            acc[za, :, cols] = result[:TM]
            if zb is not None:
                acc[zb, :, cols] = result[TM:]

        wide(4, down)

    def ret_copy(g, j, slot):
        rows = pl.ds(0, SENT[g])
        return rcopy(
            ret_s.at[g, j, rows], ret_r.at[g, slot, rows], ret_ss.at[g, j], ret_rs.at[g, slot],
            peer(j),
        )

    def give_back(g, placed):
        height = placed.shape[0] // NE

        def down(cols):
            result = dot(placed, wd[:, cols]).astype(BF16)
            ret_s[g, :, pl.ds(0, height), cols] = result.reshape(NE, height, D // 8)

        wide(8, down)
        over_peers(lambda j: ret_copy(g, j, me).start())
        ret_r[g, me] = ret_s[g, me]

    own_hidden = hidden(ag_r[z].reshape(ROWS, D), wr)
    give_back(0, dot(cselect_ref[...], own_hidden, ((0,), (0,))).astype(BF16))
    relay_own(2)
    shared(z)

    entry[...] = jnp.zeros_like(entry)

    def take_state(j, carry):
        @pl.when(j < me)
        def _():
            st_copy(j, j).wait_recv()
            sums = st_r[j, pl.ds(BLOCK, 16), :].astype(F32)
            decay = jnp.exp(sums[0:1] + sums[1:2] + sums[2:3])
            entry[...] = decay * entry[...] + st_r[j, pl.ds(0, BLOCK), :].astype(F32)

        return carry


    def retain(n, carry):
        rows = pl.ds(pl.multiple_of(n * BLOCK, BLOCK), BLOCK)
        row = run_s[pl.ds(n, 1), :]
        spread = along(row)
        query, key, value = turned(q_ref, n), keys[rows, :], v_ref[rows, :]
        scores = dot(query, key, ((1,), (1,)))
        factor = jnp.exp(jnp.where(lower, spread - row, 0.0))
        mixed = jnp.where(lower, scores * factor, 0.0).astype(BF16)
        scaled_query = (query.astype(F32) * jnp.exp(spread)).astype(BF16)
        offset = jnp.exp(off_s[pl.ds(n, 1), :][:, 0:1])
        prior = (before[n] + offset * entry[...]).astype(BF16)
        kept = dot(mixed, value) + dot(scaled_query, prior)
        scale = lax.rsqrt(jnp.mean(kept * kept, axis=-1, keepdims=True) + epsilon)
        gated = (silu(g_ref[rows, :].astype(F32)) * (kept * scale)).astype(BF16)

        def project(cols):
            term = dot(gated, ow_ref[:, cols]).astype(BF16)
            mix[0, n, :, cols] = term[:64]
            mix[1, n, :, cols] = term[64:]

        wide(4, project)
        return carry

    mix_copy = rcopy(mix.at[pc], mixp, mixp_s, mixp_r, partner)

    for h in (1, 2, 3):
        za, zb = zat(-h), zat(h)
        for k in (0, 1):
            for way in (0, 1):
                ag_wait(way, h - 1, CR0 + k)
            for way in (0, 1):
                if h < 3 or way == k:
                    ag_start(way, h, CR0 + k)
            h_rows = hidden(jnp.concatenate([ag_r[za, k], ag_r[zb, k]], axis=0), wr)
            hid[0, pl.ds(k * HALF, HALF)] = h_rows[:HALF]
            hid[1, pl.ds(k * HALF, HALF)] = h_rows[HALF:]
        if h < 3:
            placed = dot(cperm_ref[:, pl.ds(0, 2 * ROWS)], hid[pl.ds(0, 2)].reshape(2 * ROWS, 256))
        else:
            ag_wait(0, 3, CR0)
            ag_wait(1, 3, CR1)
            hid[2] = hidden(ag_r[zat(4)].reshape(ROWS, D), wr)
            placed = dot(cperm_ref[...], hid[...].reshape(3 * ROWS, 256))
        give_back(h, placed.astype(BF16))
        shared(za, zb)
        if h == 1:
            for copy in arriving[6:9]:
                copy.wait()
            lax.fori_loop(0, NE - 1, take_state, 0)
            lax.fori_loop(0, NZ // 2, retain, 0)
        if h == 2:
            lax.fori_loop(NZ // 2, NZ, retain, 0)
            mix_copy.start()
    ag_wait(0, 3, CO)
    ag_wait(1, 3, CM)
    shared(zat(4))

    def chain(base, send, recv, ss, rs):
        half = D // 2

        def copy(way, s, part):
            dev = {"z": zup if way == 0 else zdown}
            cols = pl.ds(part * half, half)
            return rcopy(
                send.at[way, s, :, cols], recv.at[way, s, :, cols], ss.at[way, s, part],
                rs.at[way, s, part], dev,
            )

        def forward(way, s, part):
            target = zat(4 - s if way == 0 else s - 4)
            cols = pl.ds(part * half, half)
            value = base(target, cols)
            if s > (0 if part == way else 1):
                copy(way, s - 1, part).wait_recv()
                value = value + recv[way, s - 1, :, cols].astype(F32)
            send[way, s, :, cols] = value.astype(BF16)
            copy(way, s, part).start()

        def step(s):
            for way in (0, 1):
                forward(way, s, way)
            if s < 3:
                for way in (0, 1):
                    forward(way, s + 1, 1 - way)

        def finish(out_ref):
            for part in (0, 1):
                cols = pl.ds(part * half, half)
                value = base(z, cols)
                for way in (0, 1):
                    copy(way, 3, part).wait_recv()
                    value = value + recv[way, 3, :, cols].astype(F32)
                out_ref[:, cols] = value.astype(BF16)

        def drain():
            for way in (0, 1):
                for s in range(4):
                    for part in (0, 1):
                        if s or part == way:
                            copy(way, s, part).wait_send()

        return step, finish, drain

    def mix_base(target, cols):
        return mix[c, target, :, cols].astype(F32) + mixp[target, :, cols].astype(F32)

    def moe_base(target, cols):
        return acc[target, :, cols] + othp[target, :, cols].astype(F32)

    mix_step, mix_finish, mix_drain = chain(mix_base, rm_s, rm_r, rm_ss, rm_rs)
    moe_step, moe_finish, moe_drain = chain(moe_base, rs_s, rs_r, rs_ss, rs_rs)

    sources = [
        (0, 0, 0), (1, 0, -1), (1, 1, 1), (2, 0, -2), (2, 1, 2), (3, 2, 4), (3, 0, -3), (3, 1, 3)
    ]

    def oth_copy(n):
        where = zat(sources[n][2])
        return rcopy(oth.at[where], othp.at[where], oth_s.at[n], oth_r.at[n], partner)

    def combine(g):
        over_peers(lambda j: ret_copy(g, j, j).wait_recv())
        for n, (group, zi, offset) in enumerate(sources):
            if group != g:
                continue
            where = zat(offset)
            weight = ag_m[where]
            table = [ccomb0_ref[rel] if g == 0 else ccomb_ref[zi, rel] for rel in (0, 1)]
            spread = jnp.concatenate(
                [dot(weight[:TM], table[0]), dot(weight[TM:], table[1])], axis=0
            ).astype(BF16)
            height = PAD if g == 0 else RET

            def gather(cols):
                rows = ret_r[g, :, pl.ds(0, height), cols].reshape(NE * height, D // 4)
                result = dot(spread, rows)
                acc[where, :, cols] += result[:TM]
                oth[where, :, cols] = result[TM:].astype(BF16)

            wide(4, gather)
            oth_copy(n).start()

    for copy in arriving[10:]:
        copy.wait()
    mix_copy.wait_recv()
    mix_step(0)
    combine(0)
    combine(1)
    mix_step(1)
    combine(2)
    mix_step(2)
    mix_step(3)
    combine(3)
    for n in range(NZ):
        oth_copy(n).wait_recv()
    moe_step(0)
    mix_finish(mixer_ref)
    for s in (1, 2, 3):
        moe_step(s)
    moe_finish(channel_ref)

    for copy in pair + sent + [mix_copy]:
        copy.wait_send()
    over_peers(lambda j: a2a_copy(j, me).wait_send())
    each_later(lambda j: st_copy(j, me).wait_send())
    for way in (0, 1):
        ag_copy(way, 0, CO, z, first=True).wait_send()
        for hop in range(3):
            for chunk in (CO, CM, CR0, CR1):
                if hop or chunk != CO:
                    ag_copy(way, hop, chunk, z).wait_send()
    for way, chunk in ((0, CO), (1, CM), (0, CR0), (1, CR1)):
        ag_copy(way, 3, chunk, z).wait_send()
    for g in range(4):
        over_peers(lambda j: ret_copy(g, j, me).wait_send())
    for n in range(NZ):
        oth_copy(n).wait_send()
    mix_drain()
    moe_drain()


def fused(*args):
    vmem = pl.BlockSpec(memory_space=pltpu.VMEM)
    hbm = pl.BlockSpec(memory_space=pl.ANY)
    sem = pltpu.SemaphoreType.DMA
    scratch = [
        pltpu.VMEM(s, t)
        for s, t in (
            ((1024, 128), BF16), ((1024, 128), BF16), ((1024, 256), BF16), ((1024, 256), BF16),
            ((NZ, BLOCK), F32), ((256, D), BF16),
            ((2, NE * PAD, 128), BF16), ((3, 2, 128, NE * RET), BF16), ((2, 128, NE * PAD), BF16),
            ((ROWS, NE * PAD), BF16), ((NE * RET, 3 * ROWS), BF16), ((4, 128, 128), F32),
            ((TM, D), BF16), ((4, TM, 128), BF16), ((1024, 128), BF16),
            ((2, D, 256), BF16), ((256, D), BF16), ((2, D, 256), BF16), ((256, D), BF16),
            ((TM, D), BF16), ((2, TM, 128), BF16),
            ((NE, PAD, D), BF16), ((NE, PAD, D), BF16),
            ((NZ, TM, D), BF16), ((NZ, 2 * TM, 128), BF16), ((NZ, 2, HALF, D), BF16),
            ((3, ROWS, 256), BF16),
            ((4, NE, RET, D), BF16), ((4, NE, RET, D), BF16),
            ((NZ, TM, D), F32), ((NZ, TM, D), BF16), ((NZ, TM, D), BF16),
            ((2, NZ, 64, D), BF16), ((NZ, 64, D), BF16),
            ((2, 4, TM, D), BF16), ((2, 4, TM, D), BF16),
            ((2, 4, 64, D), BF16), ((2, 4, 64, D), BF16),
            ((144, 256), BF16), ((NE, 144, 256), BF16),
            ((NZ, BLOCK, 256), F32), ((BLOCK, 256), F32), ((BLOCK, 256), F32),
            ((NZ, BLOCK), F32), ((NZ, BLOCK), F32),
        )
    ] + [
        sem((12,)), sem((6,)), sem((6,)), sem((6,)), sem((3,)), sem((3,)), sem((NE,)), sem((NE,)),
        sem((2, 4, 4)), sem((2, 4, 4)), sem((NE,)), sem((NE,)),
        sem((4, NE)), sem((4, NE)), sem((NZ,)), sem((NZ,)), sem, sem,
        sem((2, 4, 2)), sem((2, 4, 2)), sem((2, 4, 2)), sem((2, 4, 2)),
    ]
    return pl.pallas_call(
        kernel,
        out_shape=(jax.ShapeDtypeStruct((64, D), BF16), jax.ShapeDtypeStruct((TM, D), BF16)),
        in_specs=[vmem] * 4 + [hbm] * 18,
        out_specs=(vmem, vmem),
        scratch_shapes=scratch,
        compiler_params=pltpu.CompilerParams(
            collective_id=0, has_side_effects=True, vmem_limit_bytes=67043328
        ),
    )(*args)


def local(
    query_rows, key_rows, value_rows, gate_rows, log_decay, out_weight, channel_input, norm_gain,
    routes, route_weight, expert_gate, expert_up, expert_down, shared_gate, shared_up, shared_down,
):
    return fused(
        channel_input, norm_gain.reshape(1, D), routes, route_weight,
        query_rows, key_rows, value_rows, gate_rows, log_decay.reshape(NZ, BLOCK), out_weight,
        expert_gate, expert_up, expert_down, shared_gate, shared_up, shared_down,
        *constants(),
    )


def solution(mesh):
    split = Mesh(mesh.devices.reshape(4, 4, NZ, 2), ALL)
    return jax.shard_map(
        local,
        mesh=split,
        in_specs=(
            P(EP, TP), P(EP, TP), P(EP, TP), P(EP, TP), P(TP, EP), P(TP, None),
            P(ALL, None), P(), P(ALL, None), P(ALL, None),
            P(EP, None, TP), P(EP, None, TP), P(EP, TP, None),
            P(None, TP), P(None, TP), P(TP, None),
        ),
        out_specs=(P(ALL, None), P(ALL, None)),
        check_vma=False,
    )
```

time: 187 us -> 159 us (0.85)
  the two profiles are of different devices: /device:TPU:24 before, /device:TPU:10 now
where the time goes in v2:
time: 159 us; the launch traced here: 158 us
  Pallas kernels  153 us (96%)
  local copies, waits for them, and re-layouts  4.46 us (3%)
    pallas_call x1, Pallas kernels, fused(): pl.pallas_call(kernel, out_shape=(jax.ShapeDtypeStruct((64, D), BF16), ja...  153 us
    unnamed x10, local copies, waits for them, and re-layouts  4.46 us

profile of v2, /device:TPU:10, one launch (start us, length us, event | category | flops | bytes accessed | tf_op | source)
XLA Modules:
  0.0 158.5 jit_solution(14366808947029967794)
XLA Ops:
  0.6 0.0 copy-start.1
  0.6 0.7 copy-done.1
  1.3 0.0 copy-start.2
  1.3 0.7 copy.24.routes_ref
  2.0 0.0 copy-done.2
  2.0 0.7 copy.25.share_ref
  2.7 153.4 %shard_map.221 = (bf16[64,2048]{1,0:T(8,128)(2,1)}, bf16[48,2048]{1,0:T(8,128)(2,1)}) custom-call(bf16[48,2048]{1,0:T(8,128)(2,1)} %chan_ref.1, f32[1,2048]{1,0:T(1,128)} %bitcast.2, s32[48,2]{1,0:T(8,128)} %copy.24.routes_ref, f32[48,2]{1,0:T(8,128)} %copy.25.share_ref, bf16[1024,128]{1,0:T(8,128)(2,1)} %q_hbm.1, bf16[1024,128]{1,0:T(8,128)(2,1)} %k_hbm.1, ...), custom_call_target="tpu_custom_call" | custom-call | tf_op jit(solution)/shard_map/pallas_call | solution.py:582
  156.1 0.0 copy-start
  156.1 1.7 %copy.28 = bf16[64,2048]{1,0:T(8,128)(2,1)} copy(bf16[64,2048]{1,0:T(8,128)(2,1)} %get-tuple-element.4) | data formatting | bytes 524288
  157.8 0.0 copy-done
  157.8 0.7 copy.29
Async XLA Ops:
  0.6 0.7 copy-start.1
  1.3 0.7 copy-start.2
  156.1 1.7 %copy-start = (bf16[48,2048]{1,0:T(8,128)(2,1)S(1)}, bf16[48,2048]{1,0:T(8,128)(2,1)}, u32[]{:S(2)}) copy-start(bf16[48,2048]{1,0:T(8,128)(2,1)} %get-tuple-element.5) | copy-start | bytes 589828

commit v3 on v2

--- a/solution.py
+++ b/solution.py
@@ -28,13 +28,15 @@
 ROWS = NE * PAIR
 HALF = ROWS // 2
 PAD = 16
-RET = 32
 CO, CM, CR0, CR1 = 0, 1, 2, 3
-SENT = (16, 24, 24, 32)
-ORDER = (
-    (2, 2), (3, 2), (2, 3), (1, 2), (2, 1), (2, 0), (0, 2), (3, 1), (1, 3), (3, 3), (1, 1),
-    (3, 0), (0, 3), (1, 0), (0, 1),
+PARCELS = ((0, 0, 16), (1, 0, 16), (1, 16, 24), (2, 0, 16), (2, 16, 16))
+HEIGHTS = (16, 48, 32)
+BLOCKS = (
+    (0, 0), (2, 2), (2, 0), (0, 2), (3, 1), (1, 3), (3, 3), (1, 1),
+    (3, 2), (2, 3), (1, 2), (2, 1), (3, 0), (0, 3), (1, 0), (0, 1),
 )
+BACK = tuple(BLOCKS.index((-dy % 4, -dx % 4)) for dy, dx in BLOCKS)
+HB = NE // 2
 
 
 def dot(a, b, dims=None, precision=None):
@@ -49,38 +51,44 @@
 
 def constants():
     place = np.zeros((2, NE * PAD, 128), np.float32)
-    comb = np.zeros((3, 2, 128, NE * RET), np.float32)
-    comb_own = np.zeros((2, 128, NE * PAD), np.float32)
-    select = np.zeros((ROWS, NE * PAD), np.float32)
-    perm = np.zeros((NE * RET, 3 * ROWS), np.float32)
+    select = np.zeros((HALF, HB * PAD), np.float32)
+    near_first = np.zeros((HB * 16, 2 * HALF), np.float32)
+    near_rest = np.zeros((HB * 32, 4 * HALF), np.float32)
+    far_first = np.zeros((HB * 16, 2 * HALF), np.float32)
+    far_rest = np.zeros((HB * 16, 3 * HALF), np.float32)
     for j in range(NE):
         for rel in range(2):
             for p in range(CAP):
-                comb_own[rel, j * CAP + p, j * PAD + rel * CAP + p] = 1
                 place[rel, j * PAD + rel * CAP + p, j * CAP + p] = 1
-                for zi in range(3):
-                    comb[zi, rel, j * CAP + p, j * RET + zi * PAIR + rel * CAP + p] = 1
+    for b in range(HB):
         for r in range(PAIR):
-            select[j * PAIR + r, j * PAD + r] = 1
-            for zi in range(3):
-                perm[j * RET + zi * PAIR + r, zi * ROWS + j * PAIR + r] = 1
+            select[b * PAIR + r, b * PAD + r] = 1
+            for zi in range(4):
+                row, column = zi * PAIR + r, zi * HALF + b * PAIR + r
+                if row < 16:
+                    near_first[b * 16 + row, column] = far_first[b * 16 + row, column] = 1
+                else:
+                    near_rest[b * 32 + row - 16, column] = 1
+                    if zi < 3:
+                        far_rest[b * 16 + row - 16, column] = 1
     rate = turn_base ** (-(np.arange(128) % 64) / 64.0)
     near = np.arange(BLOCK)[:, None] * rate
     far = np.arange(128)[:, None] * float(BLOCK) * rate
     turns = np.stack([np.cos(near), np.sin(near), np.cos(far), np.sin(far)])
-    tables = [jnp.asarray(m, BF16) for m in (place, comb, comb_own, select, perm)]
-    return tables + [jnp.asarray(turns, F32)]
+    tables = (place, select, near_first, near_rest, far_first, far_rest)
+    return [jnp.asarray(m, BF16) for m in tables] + [jnp.asarray(turns, F32)]
 
 
 def kernel(
     chan_ref, gain_ref, routes_ref, share_ref,
     q_hbm, k_hbm, v_hbm, g_hbm, decay_hbm, ow_hbm,
     eg_ref, eu_ref, ed_ref, sg_ref, su_ref, sd_ref,
-    cplace_hbm, ccomb_hbm, ccomb0_hbm, cselect_hbm, cperm_hbm, turns_hbm,
+    cplace_hbm, cselect_hbm, near1_hbm, near2_hbm, far1_hbm, far2_hbm, turns_hbm,
     mixer_ref, channel_ref,
     q_ref, k_ref, v_ref, g_ref, decay_ref, ow_ref,
-    cplace_ref, ccomb_ref, ccomb0_ref, cselect_ref, cperm_ref, turns_ref, normed_ref, meta_ref, keys,
-    wr, wd, ws, wsd, pn, pm, outg, a2a, ag_o, ag_m, ag_r, hid, ret_s, ret_r,
+    cplace_ref, cselect_ref, near1_ref, near2_ref, far1_ref, far2_ref, turns_ref, normed_ref, meta_ref, keys,
+    wr, wd, ws, wsd, pn, pm, outg, a2a, ag_o, ag_m, ag_r, near_hid, far_hid,
+    ret0_s, ret1_s, ret2_s, ret0_r, ret1_r, ret2_r,
     acc, oth, othp, mix, mixp, rs_s, rs_r, rm_s, rm_r,
     st_s, st_r, before, state, entry, run_s, off_s,
     in_sem, load_sem, w_s, w_r, pair_s, pair_r, a2a_s, a2a_r, ag_s, ag_v, st_ss, st_rs,
@@ -98,28 +106,25 @@
     def peer(j):
         return {"y": lax.div(j, 4), "x": lax.rem(j, 4)}
 
-    others = [lax.rem(y + dy, 4) * 4 + lax.rem(x + dx, 4) for dy, dx in ORDER]
-
-    def over_peers(body):
-        for j in others:
-            body(j)
+    columns = [lax.rem(y + dy, 4) * 4 + lax.rem(x + dx, 4) for dy, dx in BLOCKS]
 
     def rcopy(src, dst, ss, rs, dev):
         return pltpu.make_async_remote_copy(
             src_ref=src, dst_ref=dst, send_sem=ss, recv_sem=rs, device_id=dev, device_id_type=MESH
         )
 
-    for g in (1, 2):
-        ret_r[g, :, pl.ds(16, 16), :] = jnp.zeros((NE, 16, D), BF16)
+    ret_s, ret_r = (ret0_s, ret1_s, ret2_s), (ret0_r, ret1_r, ret2_r)
+    ret1_r[:, pl.ds(32, 16), :] = jnp.zeros((NE, 16, D), BF16)
     barrier = pltpu.get_barrier_semaphore()
-    for j in others:
+    for j in columns[1:]:
         pl.semaphore_signal(barrier, inc=1, device_id=peer(j), device_id_type=MESH)
     for dev in ({"z": zup}, {"z": zdown}, partner):
         pl.semaphore_signal(barrier, inc=1, device_id=dev, device_id_type=MESH)
     incoming = [
         (cplace_hbm, cplace_ref), (k_hbm, k_ref), (v_hbm, v_ref), (decay_hbm, decay_ref),
         (turns_hbm, turns_ref), (cselect_hbm, cselect_ref), (q_hbm, q_ref), (g_hbm, g_ref),
-        (ow_hbm, ow_ref), (cperm_hbm, cperm_ref), (ccomb0_hbm, ccomb0_ref), (ccomb_hbm, ccomb_ref),
+        (ow_hbm, ow_ref), (near1_hbm, near1_ref), (near2_hbm, near2_ref), (far1_hbm, far1_ref),
+        (far2_hbm, far2_ref),
     ]
     arriving = [pltpu.make_async_copy(s, d, in_sem.at[n]) for n, (s, d) in enumerate(incoming)]
     for copy in arriving:
@@ -128,22 +133,32 @@
     wide_rows = chan_ref[...].astype(F32)
     mean = jnp.mean(wide_rows * wide_rows, axis=-1, keepdims=True)
     normed_ref[...] = (wide_rows * lax.rsqrt(mean + epsilon) * gain_ref[...]).astype(BF16)
-    lanes = lax.broadcasted_iota(jnp.int32, (TM, 128), 1)
-    picks = [routes_ref[:, k : k + 1] for k in (0, 1)]
+    lanes = lax.broadcasted_iota(jnp.int32, (TM, 128), 1).astype(F32)
+    token_r = lax.broadcasted_iota(jnp.int32, (TM, TM), 0)
+    token_c = lax.broadcasted_iota(jnp.int32, (TM, TM), 1)
+    unit = (token_r == token_c).astype(F32)
+
+    def upright(rows):
+        flipped = lax.dot_general(
+            unit, rows, (((1,), (1,)), ((), ())), precision=lax.Precision.HIGHEST,
+            preferred_element_type=F32,
+        )
+        return [flipped[:, k : k + 1] for k in (0, 1)]
+
+    picks = upright(routes_ref[...].astype(F32))
+    gains = upright(share_ref[...])
     hits = [(lanes == pick).astype(F32) for pick in picks]
-    strict = lax.broadcasted_iota(jnp.int32, (TM, TM), 0) > lax.broadcasted_iota(
-        jnp.int32, (TM, TM), 1
-    )
+    strict = token_r > token_c
     earlier = dot(strict.astype(F32).astype(BF16), (hits[0] + hits[1]).astype(BF16))
     metas = [jnp.zeros((TM, 128), F32)] * 4
     for k in (0, 1):
         rank = jnp.sum(earlier * hits[k], axis=-1, keepdims=True)
-        slot = (picks[k] >> 1).astype(F32) * CAP + rank
-        there = (lanes.astype(F32) == slot).astype(F32)
+        column = jnp.floor(picks[k] * 0.5)
+        there = (lanes == column * CAP + rank).astype(F32)
         for parity in (0, 1):
-            mine = there * ((picks[k] & 1) == parity).astype(F32)
+            mine = there * (picks[k] - 2 * column == parity).astype(F32)
             metas[parity] += mine
-            metas[2 + parity] += mine * share_ref[:, k : k + 1]
+            metas[2 + parity] += mine * gains[k]
     for n in range(4):
         meta_ref[n] = metas[n].astype(BF16)
     pl.semaphore_wait(barrier, NE + 2)
@@ -190,7 +205,7 @@
         (sd_ref, wsd.at[pl.ds(0, 128)]),
     ]
     loaded = [pltpu.make_async_copy(s, d, load_sem.at[n]) for n, (s, d) in enumerate(loads)]
-    for copy in sent + loaded:
+    for copy in loaded:
         copy.start()
     ag_o[z] = normed_ref[...]
     ag_m[z, pl.ds(0, TM)] = meta_ref[2 + c]
@@ -217,11 +232,14 @@
 
     wide(4, gather_rows)
 
-    def a2a_copy(j, slot):
-        return rcopy(outg.at[j], a2a.at[slot], a2a_s.at[j], a2a_r.at[slot], peer(j))
-
-    over_peers(lambda j: a2a_copy(j, me).start())
-    a2a[me] = outg[me]
+    def a2a_copy(r, slot):
+        return rcopy(
+            outg.at[columns[r]], a2a.at[slot], a2a_s.at[r], a2a_r.at[slot], peer(columns[r])
+        )
+
+    for r in range(1, NE):
+        a2a_copy(r, BACK[r]).start()
+    a2a[0] = outg[me]
 
     def relay_own(hop):
         for chunk in (CO, CM):
@@ -285,28 +303,33 @@
         return rcopy(st_s, st_r.at[slot], st_ss.at[j], st_rs.at[slot], peer(j))
 
     def each_later(body):
-        for j in others:
+        for j in columns[1:]:
 
             @pl.when(j > me)
             def _():
                 body(j)
 
     relay_own(0)
-    relay_own(1)
-
-    over_peers(lambda j: a2a_copy(j, j).wait_recv())
-    each_later(lambda j: st_copy(j, me).start())
+    for copy in sent:
+        copy.start()
+
     arriving[5].wait()
-
-    def pack_rows(cols):
-        rows = dot(cselect_ref[...], a2a[:, :, cols].reshape(NE * PAD, D // 4))
-        ag_r[z, :, :, cols] = rows.astype(BF16).reshape(2, HALF, D // 4)
-
-    wide(4, pack_rows)
-    for chunk in (CR0, CR1):
+    for k in (0, 1):
+        for r in range(max(1, k * HB), (k + 1) * HB):
+            a2a_copy(r, r).wait_recv()
+        if k == 1:
+            each_later(lambda j: st_copy(j, me).start())
+
+        def pack_rows(cols):
+            rows = dot(cselect_ref[...], a2a[pl.ds(k * HB, HB), :, cols].reshape(HB * PAD, D // 4))
+            ag_r[z, k, :, cols] = rows.astype(BF16)
+
+        wide(4, pack_rows)
         for way in (0, 1):
-            ag_start(way, 0, chunk)
-    for copy in loaded + arriving[9:10]:
+            ag_start(way, 0, CR0 + k)
+        if k == 0:
+            relay_own(1)
+    for copy in loaded + arriving[9:]:
         copy.wait()
     for copy in sent:
         copy.wait_recv()
@@ -330,27 +353,37 @@
 
         wide(4, down)
 
-    def ret_copy(g, j, slot):
-        rows = pl.ds(0, SENT[g])
+    def ret_copy(n, r, slot):
+        buffer, first, count = PARCELS[n]
+        rows = pl.ds(first, count)
         return rcopy(
-            ret_s.at[g, j, rows], ret_r.at[g, slot, rows], ret_ss.at[g, j], ret_rs.at[g, slot],
-            peer(j),
+            ret_s[buffer].at[r, rows], ret_r[buffer].at[slot, rows], ret_ss.at[n, r],
+            ret_rs.at[n, slot], peer(columns[r]),
         )
 
-    def give_back(g, placed):
-        height = placed.shape[0] // NE
+    def give_back(n, first, count, placed):
+        buffer, top, _ = PARCELS[n]
+        height = placed.shape[0] // count
 
         def down(cols):
             result = dot(placed, wd[:, cols]).astype(BF16)
-            ret_s[g, :, pl.ds(0, height), cols] = result.reshape(NE, height, D // 8)
+            ret_s[buffer][pl.ds(first, count), pl.ds(top, height), cols] = result.reshape(
+                count, height, D // 8
+            )
 
         wide(8, down)
-        over_peers(lambda j: ret_copy(g, j, me).start())
-        ret_r[g, me] = ret_s[g, me]
+        for r in range(max(first, 1), first + count):
+            ret_copy(n, r, me).start()
+        if first == 0:
+            rows = pl.ds(top, height)
+            ret_r[buffer][me, rows] = ret_s[buffer][0, rows]
 
     own_hidden = hidden(ag_r[z].reshape(ROWS, D), wr)
-    give_back(0, dot(cselect_ref[...], own_hidden, ((0,), (0,))).astype(BF16))
-    relay_own(2)
+    own_placed = [
+        dot(cselect_ref[...], own_hidden[k * HALF : (k + 1) * HALF], ((0,), (0,))).astype(BF16)
+        for k in (0, 1)
+    ]
+    give_back(0, 0, NE, jnp.concatenate(own_placed, axis=0))
     shared(z)
 
     entry[...] = jnp.zeros_like(entry)
@@ -391,6 +424,9 @@
 
     mix_copy = rcopy(mix.at[pc], mixp, mixp_s, mixp_r, partner)
 
+    def retain_two(n):
+        lax.fori_loop(2 * n, 2 * n + 2, retain, 0)
+
     for h in (1, 2, 3):
         za, zb = zat(-h), zat(h)
         for k in (0, 1):
@@ -400,60 +436,63 @@
                 if h < 3 or way == k:
                     ag_start(way, h, CR0 + k)
             h_rows = hidden(jnp.concatenate([ag_r[za, k], ag_r[zb, k]], axis=0), wr)
-            hid[0, pl.ds(k * HALF, HALF)] = h_rows[:HALF]
-            hid[1, pl.ds(k * HALF, HALF)] = h_rows[HALF:]
+            if h == 1:
+                near_hid[k, pl.ds(0, 2 * HALF)] = h_rows
+                give_back(1, k * HB, HB, dot(near1_ref[...], h_rows).astype(BF16))
+            elif h == 2:
+                near_hid[k, pl.ds(2 * HALF, 2 * HALF)] = h_rows
+                give_back(2, k * HB, HB, dot(near2_ref[...], near_hid[k]).astype(BF16))
+            else:
+                far_hid[k, pl.ds(0, 2 * HALF)] = h_rows
+                give_back(3, k * HB, HB, dot(far1_ref[...], h_rows).astype(BF16))
+            if (h, k) == (1, 0):
+                relay_own(2)
+            if (h, k) == (1, 1):
+                for copy in arriving[6:9]:
+                    copy.wait()
+                lax.fori_loop(0, NE - 1, take_state, 0)
+                retain_two(0)
+            elif (h, k) == (2, 0):
+                retain_two(1)
+            elif (h, k) == (2, 1):
+                retain_two(2)
+            elif (h, k) == (3, 0):
+                retain_two(3)
+                mix_copy.start()
         if h < 3:
-            placed = dot(cperm_ref[:, pl.ds(0, 2 * ROWS)], hid[pl.ds(0, 2)].reshape(2 * ROWS, 256))
-        else:
-            ag_wait(0, 3, CR0)
-            ag_wait(1, 3, CR1)
-            hid[2] = hidden(ag_r[zat(4)].reshape(ROWS, D), wr)
-            placed = dot(cperm_ref[...], hid[...].reshape(3 * ROWS, 256))
-        give_back(h, placed.astype(BF16))
-        shared(za, zb)
-        if h == 1:
-            for copy in arriving[6:9]:
-                copy.wait()
-            lax.fori_loop(0, NE - 1, take_state, 0)
-            lax.fori_loop(0, NZ // 2, retain, 0)
-        if h == 2:
-            lax.fori_loop(NZ // 2, NZ, retain, 0)
-            mix_copy.start()
-    ag_wait(0, 3, CO)
-    ag_wait(1, 3, CM)
-    shared(zat(4))
-
+            shared(za, zb)
     def chain(base, send, recv, ss, rs):
-        half = D // 2
+        width = D // 4
 
         def copy(way, s, part):
             dev = {"z": zup if way == 0 else zdown}
-            cols = pl.ds(part * half, half)
+            cols = pl.ds(part * width, width)
             return rcopy(
                 send.at[way, s, :, cols], recv.at[way, s, :, cols], ss.at[way, s, part],
                 rs.at[way, s, part], dev,
             )
 
-        def forward(way, s, part):
-            target = zat(4 - s if way == 0 else s - 4)
-            cols = pl.ds(part * half, half)
-            value = base(target, cols)
-            if s > (0 if part == way else 1):
-                copy(way, s - 1, part).wait_recv()
-                value = value + recv[way, s - 1, :, cols].astype(F32)
-            send[way, s, :, cols] = value.astype(BF16)
-            copy(way, s, part).start()
+        def forward(s, part):
+            for way in (0, 1):
+                hop = s if part // 2 == way else s + 1
+                if hop > 3:
+                    continue
+                target = zat(4 - hop if way == 0 else hop - 4)
+                cols = pl.ds(part * width, width)
+                value = base(target, cols)
+                if s > 0:
+                    copy(way, hop - 1, part).wait_recv()
+                    value = value + recv[way, hop - 1, :, cols].astype(F32)
+                send[way, hop, :, cols] = value.astype(BF16)
+                copy(way, hop, part).start()
 
         def step(s):
-            for way in (0, 1):
-                forward(way, s, way)
-            if s < 3:
-                for way in (0, 1):
-                    forward(way, s + 1, 1 - way)
+            for part in (0, 2, 1, 3):
+                forward(s, part)
 
         def finish(out_ref):
-            for part in (0, 1):
-                cols = pl.ds(part * half, half)
+            for part in (0, 2, 1, 3):
+                cols = pl.ds(part * width, width)
                 value = base(z, cols)
                 for way in (0, 1):
                     copy(way, 3, part).wait_recv()
@@ -463,8 +502,8 @@
         def drain():
             for way in (0, 1):
                 for s in range(4):
-                    for part in (0, 1):
-                        if s or part == way:
+                    for part in range(4):
+                        if s or part // 2 == way:
                             copy(way, s, part).wait_send()
 
         return step, finish, drain
@@ -478,47 +517,59 @@
     mix_step, mix_finish, mix_drain = chain(mix_base, rm_s, rm_r, rm_ss, rm_rs)
     moe_step, moe_finish, moe_drain = chain(moe_base, rs_s, rs_r, rs_ss, rs_rs)
 
-    sources = [
-        (0, 0, 0), (1, 0, -1), (1, 1, 1), (2, 0, -2), (2, 1, 2), (3, 2, 4), (3, 0, -3), (3, 1, 3)
-    ]
+    sources = [(0, 0, 0), (1, 0, -1), (1, 1, 1), (1, 2, -2), (1, 3, 2), (2, 0, -3), (2, 1, 3), (2, 2, 4)]
 
     def oth_copy(n):
         where = zat(sources[n][2])
         return rcopy(oth.at[where], othp.at[where], oth_s.at[n], oth_r.at[n], partner)
 
-    def combine(g):
-        over_peers(lambda j: ret_copy(g, j, j).wait_recv())
-        for n, (group, zi, offset) in enumerate(sources):
-            if group != g:
-                continue
-            where = zat(offset)
+    def combine(buffer):
+        for n in range(5):
+            if PARCELS[n][0] == buffer:
+                for r in range(1, NE):
+                    ret_copy(n, r, columns[r]).wait_recv()
+        height = HEIGHTS[buffer]
+        lane = lax.broadcasted_iota(jnp.int32, (128, NE * height), 0).astype(F32)
+        place = lax.broadcasted_iota(jnp.int32, (128, NE * height), 1).astype(F32)
+        column = jnp.floor((lane + 0.5) * (1.0 / CAP))
+        ahead = place - (column * height + (lane - column * CAP))
+        group = [(n, zi, zat(offset)) for n, (at, zi, offset) in enumerate(sources) if at == buffer]
+        spread = []
+        for n, zi, where in group:
             weight = ag_m[where]
-            table = [ccomb0_ref[rel] if g == 0 else ccomb_ref[zi, rel] for rel in (0, 1)]
-            spread = jnp.concatenate(
-                [dot(weight[:TM], table[0]), dot(weight[TM:], table[1])], axis=0
-            ).astype(BF16)
-            height = PAD if g == 0 else RET
-
-            def gather(cols):
-                rows = ret_r[g, :, pl.ds(0, height), cols].reshape(NE * height, D // 4)
-                result = dot(spread, rows)
-                acc[where, :, cols] += result[:TM]
-                oth[where, :, cols] = result[TM:].astype(BF16)
-
-            wide(4, gather)
+            for rel in (0, 1):
+                table = (ahead == zi * PAIR + rel * CAP).astype(F32).astype(BF16)
+                spread.append(dot(weight[rel * TM : (rel + 1) * TM], table))
+        spread = jnp.concatenate(spread, axis=0).astype(BF16)
+
+        def gather(cols):
+            rows = ret_r[buffer][:, :, cols].reshape(NE * height, D // 4)
+            result = dot(spread, rows)
+            for at, (n, zi, where) in enumerate(group):
+                acc[where, :, cols] += result[2 * at * TM : (2 * at + 1) * TM]
+                oth[where, :, cols] = result[(2 * at + 1) * TM : (2 * at + 2) * TM].astype(BF16)
+
+        wide(4, gather)
+        for n, zi, where in group:
             oth_copy(n).start()
 
-    for copy in arriving[10:]:
-        copy.wait()
     mix_copy.wait_recv()
     mix_step(0)
+    opposite = zat(4)
+    for k in (0, 1):
+        ag_wait(k, 3, CR0 + k)
+        far_hid[k, pl.ds(2 * HALF, HALF)] = hidden(ag_r[opposite, k], wr)
+        give_back(4, k * HB, HB, dot(far2_ref[...], far_hid[k]).astype(BF16))
+    shared(zat(-3), zat(3))
+    mix_step(1)
+    ag_wait(0, 3, CO)
+    ag_wait(1, 3, CM)
+    shared(opposite)
     combine(0)
+    mix_step(2)
     combine(1)
-    mix_step(1)
+    mix_step(3)
     combine(2)
-    mix_step(2)
-    mix_step(3)
-    combine(3)
     for n in range(NZ):
         oth_copy(n).wait_recv()
     moe_step(0)
@@ -529,7 +580,8 @@
 
     for copy in pair + sent + [mix_copy]:
         copy.wait_send()
-    over_peers(lambda j: a2a_copy(j, me).wait_send())
+    for r in range(1, NE):
+        a2a_copy(r, r).wait_send()
     each_later(lambda j: st_copy(j, me).wait_send())
     for way in (0, 1):
         ag_copy(way, 0, CO, z, first=True).wait_send()
@@ -539,8 +591,9 @@
                     ag_copy(way, hop, chunk, z).wait_send()
     for way, chunk in ((0, CO), (1, CM), (0, CR0), (1, CR1)):
         ag_copy(way, 3, chunk, z).wait_send()
-    for g in range(4):
-        over_peers(lambda j: ret_copy(g, j, me).wait_send())
+    for g in range(5):
+        for r in range(1, NE):
+            ret_copy(g, r, me).wait_send()
     for n in range(NZ):
         oth_copy(n).wait_send()
     mix_drain()
@@ -556,15 +609,16 @@
         for s, t in (
             ((1024, 128), BF16), ((1024, 128), BF16), ((1024, 256), BF16), ((1024, 256), BF16),
             ((NZ, BLOCK), F32), ((256, D), BF16),
-            ((2, NE * PAD, 128), BF16), ((3, 2, 128, NE * RET), BF16), ((2, 128, NE * PAD), BF16),
-            ((ROWS, NE * PAD), BF16), ((NE * RET, 3 * ROWS), BF16), ((4, 128, 128), F32),
+            ((2, NE * PAD, 128), BF16), ((HALF, HB * PAD), BF16),
+            ((HB * 16, 2 * HALF), BF16), ((HB * 32, 4 * HALF), BF16), ((HB * 16, 2 * HALF), BF16),
+            ((HB * 16, 3 * HALF), BF16), ((4, 128, 128), F32),
             ((TM, D), BF16), ((4, TM, 128), BF16), ((1024, 128), BF16),
             ((2, D, 256), BF16), ((256, D), BF16), ((2, D, 256), BF16), ((256, D), BF16),
             ((TM, D), BF16), ((2, TM, 128), BF16),
             ((NE, PAD, D), BF16), ((NE, PAD, D), BF16),
             ((NZ, TM, D), BF16), ((NZ, 2 * TM, 128), BF16), ((NZ, 2, HALF, D), BF16),
-            ((3, ROWS, 256), BF16),
-            ((4, NE, RET, D), BF16), ((4, NE, RET, D), BF16),
+            ((2, 4 * HALF, 256), BF16), ((2, 3 * HALF, 256), BF16),
+            *(((NE, n, D), BF16) for n in HEIGHTS + HEIGHTS),
             ((NZ, TM, D), F32), ((NZ, TM, D), BF16), ((NZ, TM, D), BF16),
             ((2, NZ, 64, D), BF16), ((NZ, 64, D), BF16),
             ((2, 4, TM, D), BF16), ((2, 4, TM, D), BF16),
@@ -574,15 +628,15 @@
             ((NZ, BLOCK), F32), ((NZ, BLOCK), F32),
         )
     ] + [
-        sem((12,)), sem((6,)), sem((6,)), sem((6,)), sem((3,)), sem((3,)), sem((NE,)), sem((NE,)),
+        sem((13,)), sem((6,)), sem((6,)), sem((6,)), sem((3,)), sem((3,)), sem((NE,)), sem((NE,)),
         sem((2, 4, 4)), sem((2, 4, 4)), sem((NE,)), sem((NE,)),
-        sem((4, NE)), sem((4, NE)), sem((NZ,)), sem((NZ,)), sem, sem,
-        sem((2, 4, 2)), sem((2, 4, 2)), sem((2, 4, 2)), sem((2, 4, 2)),
+        sem((5, NE)), sem((5, NE)), sem((NZ,)), sem((NZ,)), sem, sem,
+        sem((2, 4, 4)), sem((2, 4, 4)), sem((2, 4, 4)), sem((2, 4, 4)),
     ]
     return pl.pallas_call(
         kernel,
         out_shape=(jax.ShapeDtypeStruct((64, D), BF16), jax.ShapeDtypeStruct((TM, D), BF16)),
-        in_specs=[vmem] * 4 + [hbm] * 18,
+        in_specs=[vmem] * 4 + [hbm] * 19,
         out_specs=(vmem, vmem),
         scratch_shapes=scratch,
         compiler_params=pltpu.CompilerParams(
@@ -596,7 +650,7 @@
     routes, route_weight, expert_gate, expert_up, expert_down, shared_gate, shared_up, shared_down,
 ):
     return fused(
-        channel_input, norm_gain.reshape(1, D), routes, route_weight,
+        channel_input, norm_gain.reshape(1, D), routes.T, route_weight.T,
         query_rows, key_rows, value_rows, gate_rows, log_decay.reshape(NZ, BLOCK), out_weight,
         expert_gate, expert_up, expert_down, shared_gate, shared_up, shared_down,
         *constants(),

time: 159 us -> 139 us (0.87)
  the two profiles are of different devices: /device:TPU:10 before, /device:TPU:2 now
where the time goes in v3:
time: 139 us; the launch traced here: 138 us
  Pallas kernels  135 us (97%)
  local copies, waits for them, and re-layouts  2.39 us (2%)
    pallas_call x1, Pallas kernels, fused(): pl.pallas_call(kernel, out_shape=(jax.ShapeDtypeStruct((64, D), BF16), ja...  135 us

profile of v3, /device:TPU:2, one launch (start us, length us, event | category | flops | bytes accessed | tf_op | source)
XLA Modules:
  0.0 138.5 jit_solution(13728634632550285603)
XLA Ops:
  0.6 135.5 %shard_map.230 = (bf16[64,2048]{1,0:T(8,128)(2,1)}, bf16[48,2048]{1,0:T(8,128)(2,1)}) custom-call(bf16[48,2048]{1,0:T(8,128)(2,1)} %chan_ref.1, f32[1,2048]{1,0:T(1,128)} %bitcast.4, s32[2,48]{1,0:T(2,128)} %bitcast.6, f32[2,48]{1,0:T(2,128)} %bitcast.7, bf16[1024,128]{1,0:T(8,128)(2,1)} %q_hbm.1, bf16[1024,128]{1,0:T(8,128)(2,1)} %k_hbm.1, ...), custom_call_target="tpu_custom_call" | custom-call | tf_op jit(solution)/shard_map/pallas_call | solution.py:636
  136.1 0.0 copy-start
  136.1 1.7 %copy.27 = bf16[64,2048]{1,0:T(8,128)(2,1)} copy(bf16[64,2048]{1,0:T(8,128)(2,1)} %get-tuple-element.4) | data formatting | bytes 524288
  137.8 0.0 copy-done
  137.8 0.7 copy.28
Async XLA Ops:
  136.1 1.7 %copy-start = (bf16[48,2048]{1,0:T(8,128)(2,1)S(1)}, bf16[48,2048]{1,0:T(8,128)(2,1)}, u32[]{:S(2)}) copy-start(bf16[48,2048]{1,0:T(8,128)(2,1)} %get-tuple-element.5) | copy-start | bytes 589828

commit v4 on v3

--- a/solution.py
+++ b/solution.py
@@ -32,8 +32,8 @@
 PARCELS = ((0, 0, 16), (1, 0, 16), (1, 16, 24), (2, 0, 16), (2, 16, 16))
 HEIGHTS = (16, 48, 32)
 BLOCKS = (
-    (0, 0), (2, 2), (2, 0), (0, 2), (3, 1), (1, 3), (3, 3), (1, 1),
-    (3, 2), (2, 3), (1, 2), (2, 1), (3, 0), (0, 3), (1, 0), (0, 1),
+    (0, 0), (2, 2), (0, 2), (2, 0), (1, 3), (3, 1), (3, 3), (1, 1),
+    (2, 3), (3, 2), (2, 1), (1, 2), (0, 3), (3, 0), (0, 1), (1, 0),
 )
 BACK = tuple(BLOCKS.index((-dy % 4, -dx % 4)) for dy, dx in BLOCKS)
 HB = NE // 2
@@ -80,11 +80,12 @@
 
 
 def kernel(
-    chan_ref, gain_ref, routes_ref, share_ref,
+    chan_hbm, gain_hbm, routes_hbm, share_hbm,
     q_hbm, k_hbm, v_hbm, g_hbm, decay_hbm, ow_hbm,
     eg_ref, eu_ref, ed_ref, sg_ref, su_ref, sd_ref,
     cplace_hbm, cselect_hbm, near1_hbm, near2_hbm, far1_hbm, far2_hbm, turns_hbm,
     mixer_ref, channel_ref,
+    chan_ref, gain_ref, routes_ref, share_ref, first_sem,
     q_ref, k_ref, v_ref, g_ref, decay_ref, ow_ref,
     cplace_ref, cselect_ref, near1_ref, near2_ref, far1_ref, far2_ref, turns_ref, normed_ref, meta_ref, keys,
     wr, wd, ws, wsd, pn, pm, outg, a2a, ag_o, ag_m, ag_r, near_hid, far_hid,
@@ -113,6 +114,12 @@
             src_ref=src, dst_ref=dst, send_sem=ss, recv_sem=rs, device_id=dev, device_id_type=MESH
         )
 
+    firsts = [
+        (chan_hbm, chan_ref), (gain_hbm, gain_ref), (routes_hbm, routes_ref), (share_hbm, share_ref),
+    ]
+    firsts = [pltpu.make_async_copy(s, d, first_sem.at[n]) for n, (s, d) in enumerate(firsts)]
+    for copy in firsts:
+        copy.start()
     ret_s, ret_r = (ret0_s, ret1_s, ret2_s), (ret0_r, ret1_r, ret2_r)
     ret1_r[:, pl.ds(32, 16), :] = jnp.zeros((NE, 16, D), BF16)
     barrier = pltpu.get_barrier_semaphore()
@@ -130,6 +137,8 @@
     for copy in arriving:
         copy.start()
 
+    for copy in firsts:
+        copy.wait()
     wide_rows = chan_ref[...].astype(F32)
     mean = jnp.mean(wide_rows * wide_rows, axis=-1, keepdims=True)
     normed_ref[...] = (wide_rows * lax.rsqrt(mean + epsilon) * gain_ref[...]).astype(BF16)
@@ -317,7 +326,7 @@
     for k in (0, 1):
         for r in range(max(1, k * HB), (k + 1) * HB):
             a2a_copy(r, r).wait_recv()
-        if k == 1:
+        if k == 0:
             each_later(lambda j: st_copy(j, me).start())
 
         def pack_rows(cols):
@@ -368,10 +377,10 @@
         def down(cols):
             result = dot(placed, wd[:, cols]).astype(BF16)
             ret_s[buffer][pl.ds(first, count), pl.ds(top, height), cols] = result.reshape(
-                count, height, D // 8
+                count, height, D // 4
             )
 
-        wide(8, down)
+        wide(4, down)
         for r in range(max(first, 1), first + count):
             ret_copy(n, r, me).start()
         if first == 0:
@@ -424,8 +433,8 @@
 
     mix_copy = rcopy(mix.at[pc], mixp, mixp_s, mixp_r, partner)
 
-    def retain_two(n):
-        lax.fori_loop(2 * n, 2 * n + 2, retain, 0)
+    def retain_some(first, last):
+        lax.fori_loop(first, last, retain, 0)
 
     for h in (1, 2, 3):
         za, zb = zat(-h), zat(h)
@@ -447,20 +456,20 @@
                 give_back(3, k * HB, HB, dot(far1_ref[...], h_rows).astype(BF16))
             if (h, k) == (1, 0):
                 relay_own(2)
-            if (h, k) == (1, 1):
+                shared(za, zb)
+            elif (h, k) == (1, 1):
                 for copy in arriving[6:9]:
                     copy.wait()
                 lax.fori_loop(0, NE - 1, take_state, 0)
-                retain_two(0)
+                retain_some(0, 1)
             elif (h, k) == (2, 0):
-                retain_two(1)
+                retain_some(1, 5)
             elif (h, k) == (2, 1):
-                retain_two(2)
+                shared(za, zb)
             elif (h, k) == (3, 0):
-                retain_two(3)
+                retain_some(5, 8)
                 mix_copy.start()
-        if h < 3:
-            shared(za, zb)
+
     def chain(base, send, recv, ss, rs):
         width = D // 4
 
@@ -524,10 +533,6 @@
         return rcopy(oth.at[where], othp.at[where], oth_s.at[n], oth_r.at[n], partner)
 
     def combine(buffer):
-        for n in range(5):
-            if PARCELS[n][0] == buffer:
-                for r in range(1, NE):
-                    ret_copy(n, r, columns[r]).wait_recv()
         height = HEIGHTS[buffer]
         lane = lax.broadcasted_iota(jnp.int32, (128, NE * height), 0).astype(F32)
         place = lax.broadcasted_iota(jnp.int32, (128, NE * height), 1).astype(F32)
@@ -541,6 +546,10 @@
                 table = (ahead == zi * PAIR + rel * CAP).astype(F32).astype(BF16)
                 spread.append(dot(weight[rel * TM : (rel + 1) * TM], table))
         spread = jnp.concatenate(spread, axis=0).astype(BF16)
+        for n in range(5):
+            if PARCELS[n][0] == buffer:
+                for r in range(1, NE):
+                    ret_copy(n, r, columns[r]).wait_recv()
 
         def gather(cols):
             rows = ret_r[buffer][:, :, cols].reshape(NE * height, D // 4)
@@ -605,6 +614,9 @@
     hbm = pl.BlockSpec(memory_space=pl.ANY)
     sem = pltpu.SemaphoreType.DMA
     scratch = [
+        pltpu.VMEM((TM, D), BF16), pltpu.VMEM((1, D), F32), pltpu.VMEM((2, TM), jnp.int32),
+        pltpu.VMEM((2, TM), F32), sem((4,)),
+    ] + [
         pltpu.VMEM(s, t)
         for s, t in (
             ((1024, 128), BF16), ((1024, 128), BF16), ((1024, 256), BF16), ((1024, 256), BF16),
@@ -635,12 +647,12 @@
     ]
     return pl.pallas_call(
         kernel,
-        out_shape=(jax.ShapeDtypeStruct((64, D), BF16), jax.ShapeDtypeStruct((TM, D), BF16)),
-        in_specs=[vmem] * 4 + [hbm] * 19,
+        out_shape=(pltpu.VMEM((64, D), BF16), pltpu.VMEM((TM, D), BF16)),
+        in_specs=[hbm] * 23,
         out_specs=(vmem, vmem),
         scratch_shapes=scratch,
         compiler_params=pltpu.CompilerParams(
-            collective_id=0, has_side_effects=True, vmem_limit_bytes=67043328
+            collective_id=0, has_side_effects=True, vmem_limit_bytes=60000000
         ),
     )(*args)
 

time: 139 us -> 135 us (0.971)
  Pallas kernels: 135 us -> 133 us
    pallas_call x1, Pallas kernels: 135 us -> 133 us  [fused(): pl.pallas_call(kernel, out_shape=(pltpu.VMEM((64, D), BF16), pltpu.VMEM((...]
where the time goes in v4:
time: 135 us
  Pallas kernels  133 us (99%)
  local copies, waits for them, and re-layouts  1.38 us (1%)
    pallas_call x1, Pallas kernels, fused(): pl.pallas_call(kernel, out_shape=(pltpu.VMEM((64, D), BF16), pltpu.VMEM((...  133 us

profile of v4, /device:TPU:2, one launch (start us, length us, event | category | flops | bytes accessed | tf_op | source)
XLA Modules:
  0.0 134.7 jit_solution(10025244820000367993)
XLA Ops:
  0.6 132.6 %shard_map.230 = (bf16[64,2048]{1,0:T(8,128)(2,1)S(1)}, bf16[48,2048]{1,0:T(8,128)(2,1)S(1)}) custom-call(bf16[48,2048]{1,0:T(8,128)(2,1)} %chan_hbm.1, f32[1,2048]{1,0:T(1,128)} %bitcast.4, s32[2,48]{1,0:T(2,128)} %bitcast.6, f32[2,48]{1,0:T(2,128)} %bitcast.7, bf16[1024,128]{1,0:T(8,128)(2,1)} %q_hbm.1, bf16[1024,128]{1,0:T(8,128)(2,1)} %k_hbm.1, ...), custom_call_target="tpu_custom_call" | custom-call | tf_op jit(solution)/shard_map/pallas_call | solution.py:648
  133.3 0.7 copy.27
  134.0 0.7 copy.28

commit v5 on v4

--- a/solution.py
+++ b/solution.py
@@ -32,8 +32,8 @@
 PARCELS = ((0, 0, 16), (1, 0, 16), (1, 16, 24), (2, 0, 16), (2, 16, 16))
 HEIGHTS = (16, 48, 32)
 BLOCKS = (
-    (0, 0), (2, 2), (0, 2), (2, 0), (1, 3), (3, 1), (3, 3), (1, 1),
-    (2, 3), (3, 2), (2, 1), (1, 2), (0, 3), (3, 0), (0, 1), (1, 0),
+    (0, 0), (2, 2), (1, 3), (3, 1), (3, 3), (1, 1), (0, 2), (2, 0),
+    (2, 3), (2, 1), (3, 2), (1, 2), (0, 3), (0, 1), (3, 0), (1, 0),
 )
 BACK = tuple(BLOCKS.index((-dy % 4, -dx % 4)) for dy, dx in BLOCKS)
 HB = NE // 2

time: 135 us -> 133 us (0.985)
  Pallas kernels: 133 us -> 130 us
    pallas_call x1, Pallas kernels: 133 us -> 130 us  [fused(): pl.pallas_call(kernel, out_shape=(pltpu.VMEM((64, D), BF16), pltpu.VMEM((...]
where the time goes in v5:
time: 133 us; the launch traced here: 132 us
  Pallas kernels  130 us (98%)
  local copies, waits for them, and re-layouts  1.38 us (1%)
    pallas_call x1, Pallas kernels, fused(): pl.pallas_call(kernel, out_shape=(pltpu.VMEM((64, D), BF16), pltpu.VMEM((...  130 us

profile of v5, /device:TPU:2, one launch (start us, length us, event | category | flops | bytes accessed | tf_op | source)
XLA Modules:
  0.0 132.1 jit_solution(13838521575443987552)
XLA Ops:
  0.6 130.0 %shard_map.230 = (bf16[64,2048]{1,0:T(8,128)(2,1)S(1)}, bf16[48,2048]{1,0:T(8,128)(2,1)S(1)}) custom-call(bf16[48,2048]{1,0:T(8,128)(2,1)} %chan_hbm.1, f32[1,2048]{1,0:T(1,128)} %bitcast.4, s32[2,48]{1,0:T(2,128)} %bitcast.6, f32[2,48]{1,0:T(2,128)} %bitcast.7, bf16[1024,128]{1,0:T(8,128)(2,1)} %q_hbm.1, bf16[1024,128]{1,0:T(8,128)(2,1)} %k_hbm.1, ...), custom_call_target="tpu_custom_call" | custom-call | tf_op jit(solution)/shard_map/pallas_call | solution.py:648
  130.7 0.7 copy.27
  131.4 0.7 copy.28
